TPU v7x, 32 devices: a whole 2x2x4 slice. The times are simulated.
32 devices in a mesh: sp: 8 (over z, y), tp: 4 (over x, core).
Axes of the slice: x: 2, y: 2, z: 4, core: 2. Of those that a mesh axis runs over, the one named last changes fastest.
Arguments:
- layer_input: bfloat16 [6144, 2048], P('sp', 'tp'), may hold values from -6 to 6
- input_norm_gain: bfloat16 [2048], replicated, may hold values from 0.099609375 to 1.8984375
- query_weight: bfloat16 [2048, 2048], P(None, 'tp'), may hold values from -0.125 to 0.125
- forget_weight: bfloat16 [2048, 2048], P(None, 'tp'), may hold values from -0.125 to 0.125
- value_matrix: bfloat16 [2048, 2048], P(None, 'tp'), may hold values from -0.125 to 0.125
- output_gate_weight: bfloat16 [2048, 2048], P(None, 'tp'), may hold values from -0.125 to 0.125
- after_gate_weight: bfloat16 [2048, 2048], P(None, 'tp'), may hold values from -0.125 to 0.125
- before_gate_weight: bfloat16 [2048, 2048], P(None, 'tp'), may hold values from -0.125 to 0.125
- convolution_input_weight: bfloat16 [2048, 2048], P(None, 'tp'), may hold values from -0.125 to 0.125
- forget_minimum: float32 [2048], P('tp'), may hold values from 0.95 to 0.9999837
- surge_log_decay: float32 [6144, 2048], P('sp', 'tp'), may hold values from -2.2 to 0
- convolution_kernel: bfloat16 [3, 2048], P(None, 'tp'), may hold values from -4 to 4
- head_norm_gain: bfloat16 [128], replicated, may hold values from 0.099609375 to 1.8984375
- starting_state: float32 [16, 128, 128], P('tp', 'sp'), may hold values from -0.09375 to 0.09375
- recurrence_output_weight: bfloat16 [2048, 2048], P('tp'), may hold values from -0.09375 to 0.09375
- convolution_output_weight: bfloat16 [2048, 2048], P('tp'), may hold values from -0.09375 to 0.09375
- output_norm_gain: bfloat16 [2048], replicated, may hold values from 0.099609375 to 1.8984375
Outputs:
- layer_out: bfloat16 [6144, 2048], P(('sp', 'tp'))
All inputs are finite; a program needn't handle non-finite values.
Results may differ from a plain program's by a relative error of at most 0.014.
Values may be sent and summed in bfloat16 or wider, within the bound.
No kernel may reach another device: no remote copies, remote signals or barrier semaphores. Data moves between devices by JAX's collectives and lax.ppermute only.
A program may use at most 128 MiB of HBM per device.

v0:
```python
import jax
import jax.numpy as jnp
from jax import lax
from jax.sharding import PartitionSpec as P

DK = 128
DV = 128
CK = 3
BLK = 64


EPS = 1e-06
PRECISE_PRODUCT = lax.Precision.HIGHEST


def from_behind(value, axis, by):
    peers = lax.axis_size(axis)
    pairs = [(i, i + by) for i in range(peers) if 0 <= i + by < peers]
    return lax.ppermute(value, axis, pairs)


def rms_scale(value_rows):
    return lax.rsqrt(jnp.mean(value_rows * value_rows, axis=-1, keepdims=True) + EPS)


def block_pass(carry, inputs):
    latent_state, running = carry
    query_rows, key_inputs, value_rows, forget_gate_logits = inputs
    cumulative_decay = jnp.cumsum(forget_gate_logits, axis=1)
    length = query_rows.shape[1]
    causal_masking = jnp.tril(jnp.ones((length, length), dtype=bool))[None, :, :]
    query_scaled_rows = query_rows * jnp.exp(cumulative_decay)
    scaled_key = key_inputs * jnp.exp(-cumulative_decay)
    crossed_output = jnp.einsum(
        "bqy,byx->bqx", query_scaled_rows, latent_state, precision=PRECISE_PRODUCT
    )
    scores = jnp.einsum("htk,hsk->hts", query_scaled_rows, scaled_key, precision=PRECISE_PRODUCT)
    scores = jnp.where(causal_masking, scores, 0.0)
    o_intra = jnp.einsum("hts,hsv->htv", scores, value_rows, precision=PRECISE_PRODUCT)
    block_total = cumulative_decay[:, -1, :]
    latent_state = jnp.exp(block_total)[..., None] * latent_state + jnp.einsum(
        "otm,ote->ome",
        scaled_key * jnp.exp(block_total)[:, None, :],
        value_rows,
        precision=PRECISE_PRODUCT,
    )
    shifted = query_scaled_rows * jnp.exp(running)[:, None, :]
    return ((latent_state, running + block_total), (o_intra + crossed_output, shifted))


def shards(
    layer_input,
    input_norm_gain,
    query_weight,
    forget_weight,
    value_matrix,
    output_gate_weight,
    after_gate_weight,
    before_gate_weight,
    convolution_input_weight,
    forget_minimum,
    surge_log_decay,
    convolution_kernel,
    head_norm_gain,
    starting_state,
    recurrence_output_weight,
    convolution_output_weight,
    output_norm_gain,
):
    tokens_dev = layer_input.shape[0]
    heads_local = query_weight.shape[1] // DK
    blocks = tokens_dev // BLK
    weight_list = (
        query_weight,
        forget_weight,
        value_matrix,
        output_gate_weight,
        after_gate_weight,
        before_gate_weight,
        convolution_input_weight,
    )
    collected_rows = lax.all_gather(layer_input, "tp", axis=1, tiled=True)
    rows_f = collected_rows.astype(jnp.float32)
    normed = (rows_f * rms_scale(rows_f) * input_norm_gain.astype(jnp.float32)).astype(jnp.bfloat16)
    projections = tuple(
        (
            jnp.dot(normed, weight, preferred_element_type=jnp.float32).astype(jnp.bfloat16)
            for weight in weight_list
        )
    )
    query_raw, forget_raw, value_raw, outgate_raw, postgate_raw, pregate_raw, convval_raw = (
        projections
    )
    forget_single = forget_raw.astype(jnp.float32)
    forget_gate_logits = (
        jnp.logaddexp(
            jnp.log(forget_minimum), jnp.log1p(-forget_minimum) + jax.nn.log_sigmoid(forget_single)
        )
        + surge_log_decay
    )
    key_inputs = (1.0 - forget_minimum) * jax.nn.sigmoid(-forget_single)
    query_rows = jax.nn.silu(query_raw.astype(jnp.float32)) * DK ** (-0.5)

    def to_blocks(value_rows, width):
        return value_rows.reshape(blocks, BLK, heads_local, width).transpose(0, 2, 1, 3)

    zero_state = jnp.zeros((heads_local, DK, DV), jnp.float32)
    zero_total = jnp.zeros((heads_local, DK), jnp.float32)
    (local_state, local_total), (partial_output, shifted_query) = lax.scan(
        block_pass,
        (zero_state, zero_total),
        (
            to_blocks(query_rows, DK),
            to_blocks(key_inputs, DK),
            to_blocks(value_raw.astype(jnp.float32), DV),
            to_blocks(forget_gate_logits, DK),
        ),
    )
    moved_state, moved_total = (
        lax.all_to_all(local_state[None], "sp", split_axis=2, concat_axis=0, tiled=True),
        lax.all_to_all(
            local_total[None, :, :, None], "sp", split_axis=2, concat_axis=0, tiled=True
        ),
    )

    def advance(running, item):
        piece_state, piece_total = item
        return (jnp.exp(piece_total) * running + piece_state, running)

    _, entering = lax.scan(advance, starting_state, (moved_state, moved_total))
    carried_state = lax.all_to_all(entering, "sp", split_axis=0, concat_axis=2, tiled=True)[0]
    recurrence_step = partial_output + jnp.einsum(
        "aoxq,oqu->aoxu", shifted_query, carried_state, precision=PRECISE_PRODUCT
    )
    recurrence_step = recurrence_step.transpose(0, 2, 1, 3).reshape(tokens_dev, heads_local, DV)
    normed_heads = recurrence_step * rms_scale(recurrence_step) * head_norm_gain.astype(jnp.float32)
    rec_out = (
        normed_heads.reshape(tokens_dev, heads_local * DV)
        * jax.nn.silu(outgate_raw.astype(jnp.float32))
    ).astype(jnp.bfloat16)
    mixed_in = pregate_raw.astype(jnp.float32) * convval_raw.astype(jnp.float32)
    rim_rows = from_behind(mixed_in[tokens_dev - (CK - 1) :], "sp", 1)
    padded = jnp.concatenate([rim_rows, mixed_in], axis=0)
    taps_f = convolution_kernel.astype(jnp.float32)
    conv_sum = padded[0:tokens_dev] * taps_f[0]
    for offset in range(1, CK):
        conv_sum = conv_sum + padded[offset : offset + tokens_dev] * taps_f[offset]
    conv_out = (postgate_raw.astype(jnp.float32) * conv_sum).astype(jnp.bfloat16)
    mixed = lax.psum_scatter(
        jnp.dot(rec_out, recurrence_output_weight, preferred_element_type=jnp.float32)
        + jnp.dot(conv_out, convolution_output_weight, preferred_element_type=jnp.float32),
        "tp",
        scatter_dimension=0,
        tiled=True,
    )
    return (mixed * rms_scale(mixed) * output_norm_gain.astype(jnp.float32)).astype(jnp.bfloat16)


def solution(mesh):
    return jax.shard_map(
        shards,
        mesh=mesh,
        in_specs=(
            P("sp", "tp"),
            P(),
            P(None, "tp"),
            P(None, "tp"),
            P(None, "tp"),
            P(None, "tp"),
            P(None, "tp"),
            P(None, "tp"),
            P(None, "tp"),
            P("tp"),
            P("sp", "tp"),
            P(None, "tp"),
            P(),
            P("tp", "sp", None),
            P("tp", None),
            P("tp", None),
            P(),
        ),
        out_specs=P(("sp", "tp"), None),
        check_vma=False,
    )
```

profile of v0, /device:TPU:0, one launch (start us, length us, event | category | flops | bytes accessed | tf_op | source)
XLA Modules:
  0.0 328.3 jit_solution(12126143635630605461)
XLA Ops:
  10.1 30.0 %all-gather.2.cloned.1.call-done = bf16[768,2048]{1,0:T(8,128)(2,1)} async-done(((bf16[768,512]{1,0:T(8,128)(2,1)}), bf16[768,2048]{1,0:T(8,128)(2,1)}) %all-gather.2.cloned.1.call-update) | async-done | bytes 3145744 | tf_op jit(solution)/shard_map/all_gather | solution.py:82
  40.2 2.7 fusion.18
  43.0 7.2 %fusion.35 = (f32[768,512]{1,0:T(8,128)}, f32[768,512]{1,0:T(8,128)}) fusion(f32[512]{0:T(512)S(1)} %get-tuple-element.155, f32[768,512]{1,0:T(8,128)} %param.31, f32[512]{0:T(512)S(1)} %get-tuple-element.157, f32[512]{0:T(512)S(1)} %get-tuple-element.156, bf16[2048,512]{1,0:T(8,128)(2,1)} %param.24, bf16[768,2048]{1,0:T(8,128)(2,1)S(1)} %copy-done.5, ...), kind=kOutput, calls=%fused_computation.62 | convolution fusion | flops 1625948160 | bytes 9978880 | tf_op jit(solution)/shard_map/dot_general | solution.py:87
  50.2 2.7 reshape.89
  52.9 2.8 reshape.90
  55.6 5.8 %fusion.39 = f32[768,512]{1,0:T(8,128)} fusion(bf16[2048,512]{1,0:T(8,128)(2,1)} %param.23, bf16[768,2048]{1,0:T(8,128)(2,1)} %all-gather.2.cloned.1.call-done, f32[2048]{0:T(1024)S(1)} %convert_element_type.68, f32[768]{0:T(1024)S(1)} %add_rsqrt_fusion.1), kind=kOutput, calls=%fused_computation.66 | convolution fusion | flops 1619656704 | bytes 6827008 | tf_op jit(solution)/shard_map/dot_general | solution.py:87
  61.4 2.8 reshape.92
  64.1 5.5 %fusion.50 = f32[768,512]{1,0:T(8,128)} fusion(bf16[2048,512]{1,0:T(8,128)(2,1)} %param.25, bf16[768,2048]{1,0:T(8,128)(2,1)} %all-gather.2.cloned.1.call-done, f32[2048]{0:T(1024)S(1)} %convert_element_type.68, f32[768]{0:T(1024)S(1)} %add_rsqrt_fusion.1), kind=kOutput, calls=%fused_computation.95 | convolution fusion | flops 1617690624 | bytes 6827008 | tf_op jit(solution)/shard_map/dot_general | solution.py:87
  69.7 2.7 reshape.94
  72.4 4.2 %copy_bitcast_fusion.2 = (f32[12,4,64,128]{3,2,1,0:T(8,128)}, f32[12,4,64,128]{3,2,1,0:T(8,128)}) fusion(f32[12,64,4,128]{3,2,1,0:T(4,128)} %reshape.90, f32[12,64,4,128]{3,2,1,0:T(4,128)} %reshape.89), kind=kLoop, calls=%fused_computation.81 | loop fusion | bytes 6291456 | tf_op jit(solution)/shard_map/transpose | solution.py:105
  76.6 2.1 copy_bitcast_fusion
  78.7 105.6 %while.30 = (s32[]{:T(128)}, f32[4,128,128]{2,1,0:T(8,128)S(1)}, f32[4,128]{1,0:T(4,128)S(1)}, f32[12,4,64,128]{3,2,0,1:T(8,128)}, f32[12,4,64,128]{3,2,0,1:T(8,...) while((s32[]{:T(128)}, f32[4,128,128]{2,1,0:T(8,128)S(1)}, ...), condition=%wide.region_3.4_spmd.clone, body=%wide.region_1.3_spmd.clone.sunk | while | flops 153670656 | bytes 3577993 | solution.py:109
  83.9 2.0 fusion.91
  85.9 1.6 convolution_add_fusion.4
  92.7 2.0 fusion.91
  94.7 1.6 convolution_add_fusion.4
  101.5 1.9 fusion.91
  103.5 1.6 convolution_add_fusion.4
  110.3 2.0 fusion.91
  112.3 1.6 convolution_add_fusion.4
  119.1 1.9 fusion.91
  127.9 1.9 fusion.91
  129.9 1.6 convolution_add_fusion.4
  136.7 1.9 fusion.91
  145.5 1.9 fusion.91
  147.4 1.6 convolution_add_fusion.4
  154.3 2.0 fusion.91
  163.1 1.9 fusion.91
  171.9 2.0 fusion.91
  173.9 1.6 convolution_add_fusion.4
  180.7 1.9 fusion.91
  182.7 1.6 convolution_add_fusion.4
  185.0 5.5 %all-to-all-start = ((f32[1,4,128,1]{1,3,0,2:T(1,128)}), f32[1,4,128,1]{1,3,0,2:T(1,128)S(1)}, u32[]{:S(2)}, u32[]{:S(2)}) async-start(f32[1,4,128,1]{1,3,0,2:T(1,128)} %bitcast.7), calls=%async_computation | async-start | bytes 131072 | tf_op jit(solution)/shard_map/all_to_all | solution.py:121
  191.5 6.0 %all-to-all-done = f32[1,4,128,1]{1,3,0,2:T(1,128)S(1)} async-done(((f32[1,4,128,1]{1,3,0,2:T(1,128)}), f32[1,4,128,1]{1,3,0,2:T(1,128)S(1)}, u32[]{:S(2)}, u32[]{:S(2)}) %all-to-all-start) | async-done | bytes 2080 | tf_op jit(solution)/shard_map/all_to_all | solution.py:121
  197.5 3.6 %all-to-all-start.1 = ((f32[1,4,128,128]{3,1,0,2:T(4,128)}), f32[1,4,128,128]{3,1,0,2:T(4,128)S(1)}, u32[]{:S(2)}, u32[]{:S(2)}) async-start(f32[1,4,128,128]{3,1,0,2:T(4,128)} %bitcast.111), calls=%async_computation.1 | async-start | bytes 524288 | tf_op jit(solution)/shard_map/all_to_all | solution.py:120
  201.1 4.4 %convolution_convert_fusion = bf16[768,512]{1,0:T(8,128)(2,1)S(1)} fusion(bf16[2048,512]{1,0:T(8,128)(2,1)} %param.29, bf16[768,2048]{1,0:T(8,128)(2,1)} %all-gather.2.cloned.1.call-done, f32[2048]{0:T(1024)S(1)} %convert_element_type.68, f32[768]{0:T(1024)S(1)} %add_rsqrt_fusion.1), kind=kOutput, calls=%fused_computation.89 | convolution fusion | flops 1617297408 | bytes 6040576 | tf_op jit(solution)/shard_map/dot_general | solution.py:87
  205.6 3.6 %all-to-all-done.1 = f32[1,4,128,128]{3,1,0,2:T(4,128)S(1)} async-done(((f32[1,4,128,128]{3,1,0,2:T(4,128)}), f32[1,4,128,128]{3,1,0,2:T(4,128)S(1)}, u32[]{:S(2)}, u32[]{:S(2)}) %all-to-all-start.1) | async-done | bytes 262176 | tf_op jit(solution)/shard_map/all_to_all | solution.py:120
  209.2 5.7 %while.29 = (s32[]{:T(128)}, f32[4,16,128]{2,1,0:T(8,128)S(1)}, f32[8,4,16,128]{3,2,1,0:T(8,128)}, f32[8,4,16,1]{2,1,3,0:T(4,128)S(1)}, f32[8,4,16,128]{3,2,1,0:T(8,128)S(1)}, /*index=5*/s32[]{:T(128)}) while((s32[]{:T(128)}, f32[4,16,128]{2,1,0:T(8,128)S(1)}, f32[8,4,16,128]{3,2,1,0:T(8,128)}, f32[8,4,16,1]{2,1,3,0:T(4,128)S(1)}, ...), condition=%wide.region_5.6_spmd, body=%wide.region_4.5_spmd.sunk | while | flops 16386 | bytes 165197 | solution.py:130
  214.9 3.4 %all-to-all-start.2 = ((f32[8,4,16,128]{3,2,1,0:T(8,128)}), f32[8,4,16,128]{3,2,1,0:T(8,128)S(1)}, u32[]{:S(2)}, u32[]{:S(2)}) async-start(f32[8,4,16,128]{3,2,1,0:T(8,128)} %get-tuple-element.85), calls=%async_computation.2 | async-start | bytes 524288 | tf_op jit(solution)/shard_map/all_to_all | solution.py:131
  218.4 4.4 %convert_multiply_fusion.4 = f32[768,512]{1,0:T(8,128)S(1)} fusion(bf16[768,512]{1,0:T(8,128)(2,1)S(1)} %convolution_convert_fusion, bf16[2048,512]{1,0:T(8,128)(2,1)} %param.28, bf16[768,2048]{1,0:T(8,128)(2,1)} %all-gather.2.cloned.1.call-done, f32[2048]{0:T(1024)S(1)} %convert_element_type.68, f32[768]{0:T(1024)S(1)} %add_rsqrt_fusion.1), kind=kOutput, calls=%fused_computation.85 | convolution fusion | flops 1618477056 | bytes 7613440 | tf_op jit(solution)/shard_map/dot_general | solution.py:87
  223.9 3.9 %collective-permute-start = (f32[2,512]{1,0:T(2,128)S(1)}, f32[2,512]{1,0:T(2,128)S(1)}, u32[]{:S(2)}, u32[]{:S(2)}) collective-permute-start(f32[2,512]{1,0:T(2,128)S(1)} %slice.29), channel_id=1, source_target_pairs={{0,4},{4,8},{8,12},{12,16},{16,20},{20,24},{24,28},{1,5},{5,9},{9,... | collective-permute-start | bytes 12296 | tf_op jit(solution)/shard_map/ppermute | solution.py:19
  227.8 4.5 %multiply_reduce_fusion.1 = (f32[12,64,4]{1,0,2:T(8,128)S(1)}, f32[12,64,4,128]{3,1,0,2:T(8,128)}) fusion(f32[12,4,64,128]{3,2,0,1:T(8,128)} %get-tuple-element.82, f32[4,128,128,1]{2,1,3,0:T(8,128)S(1)} %bitcast.147, f32[12,4,64,128]{3,2,0,1:T(8,128)} %get-tuple-element.86), kind=kOutput, calls=%fused_computation.86 | convolution fusion | flops 605156352 | bytes 4993024 | tf_op jit(solution)/shard_map/aoxq,oqu->aoxu/dot_general | solution.py:132
  232.5 3.6 %copy.52 = f32[12,64,4,128]{3,2,1,0:T(4,128)} copy(f32[12,64,4,128]{3,1,0,2:T(8,128)} %get-tuple-element.159) | data formatting | bytes 3145728 | tf_op jit(solution)/shard_map/transpose | solution.py:135
  236.1 1.8 mul.181
  237.9 9.8 %fusion.51 = f32[768,2048]{1,0:T(8,128)} fusion(bf16[512,2048]{1,0:T(8,128)(2,1)S(1)} %copy-done, f32[96,8,4,128]{3,2,1,0:T(4,128)} %bitcast.145, f32[96,8,4,128]{3,2,1,0:T(4,128)} %bitcast.144, bf16[2048,512]{1,0:T(8,128)(2,1)} %param.26, f32[512]{0:T(512)S(1)} %broadcast_bitcast_fusion, bf16[768,2048]{1,0:T(8,128)(2,1)} %all-gather.2.cloned.1.call-done, ...), kind=kOutput, calls=%fused_computation.97 | convolution fusion | flops 3231449088 | bytes 16790528 | tf_op jit(solution)/shard_map/dot_general | solution.py:150
  247.7 12.7 %convolution_add_fusion.2 = f32[768,2048]{1,0:T(8,128)} fusion(f32[768,2048]{1,0:T(8,128)} %fusion.51, bf16[512,2048]{1,0:T(8,128)(2,1)} %param.36, f32[2,512]{1,0:T(2,128)S(1)} %collective-permute-done, f32[768,512]{1,0:T(8,128)} %copy-done.7, bf16[2048,512]{1,0:T(8,128)(2,1)} %param.27, f32[512]{0:T(512)S(1)} %bitcast.157, f32[512]{0:T(512)S(1)} %bitcast.156, ...), kind=kOutput, calls=%fused_computation.39 | convolution fusion | flops 3233415168 | bytes 21517312 | tf_op jit(solution)/shard_map/dot_general | solution.py:151
  261.1 57.4 %reduce-scatter.2.cloned.1.call-done = f32[192,2048]{1,0:T(8,128)} async-done(((f32[768,2048]{1,0:T(8,128)}), f32[192,2048]{1,0:T(8,128)}) %reduce-scatter.2.cloned.1.call-update) | async-done | bytes 1572880 | tf_op jit(solution)/shard_map/reduce_scatter | solution.py:149
  318.5 1.7 multiply_reduce_fusion
  (168 shorter events, 83.1 us)
Async XLA Ops:
  6.5 231.4 %copy-start = (bf16[512,2048]{1,0:T(8,128)(2,1)S(1)}, bf16[512,2048]{1,0:T(8,128)(2,1)}, u32[]{:S(2)}) copy-start(bf16[512,2048]{1,0:T(8,128)(2,1)} %param.35) | copy-start | bytes 6291460
  6.5 33.6 %all-gather.2.cloned.1.call-start = ((), (), s32[]{:S(2)}) async-start(), calls=%async_computation.4 | async-start | bytes 3932160 | tf_op jit(solution)/shard_map/all_gather | solution.py:82
  40.2 2.8 copy-start.5
  72.4 4.2 %copy-start.2 = (f32[12,64,4,128]{3,2,1,0:T(4,128)S(1)}, f32[12,64,4,128]{3,2,1,0:T(4,128)}, u32[]{:S(2)}) copy-start(f32[12,64,4,128]{3,2,1,0:T(4,128)} %reshape.92) | copy-start | bytes 4718596
  72.4 4.2 %copy-start.3 = (f32[12,64,4,128]{3,2,1,0:T(4,128)S(1)}, f32[12,64,4,128]{3,2,1,0:T(4,128)}, u32[]{:S(2)}) copy-start(f32[12,64,4,128]{3,2,1,0:T(4,128)} %reshape.94) | copy-start | bytes 4718596
  185.0 12.4 %all-to-all-start = ((f32[1,4,128,1]{1,3,0,2:T(1,128)}), f32[1,4,128,1]{1,3,0,2:T(1,128)S(1)}, u32[]{:S(2)}, u32[]{:S(2)}) async-start(f32[1,4,128,1]{1,3,0,2:T(1,128)} %bitcast.7), calls=%async_computation | async-start | bytes 131072 | tf_op jit(solution)/shard_map/all_to_all | solution.py:121
  197.5 11.7 %all-to-all-start.1 = ((f32[1,4,128,128]{3,1,0,2:T(4,128)}), f32[1,4,128,128]{3,1,0,2:T(4,128)S(1)}, u32[]{:S(2)}, u32[]{:S(2)}) async-start(f32[1,4,128,128]{3,1,0,2:T(4,128)} %bitcast.111), calls=%async_computation.1 | async-start | bytes 524288 | tf_op jit(solution)/shard_map/all_to_all | solution.py:120
  201.1 8.1 %copy-start.4 = (f32[4,16,128]{2,1,0:T(8,128)S(1)}, f32[4,16,128]{2,1,0:T(8,128)}, u32[]{:S(2)}) copy-start(f32[4,16,128]{2,1,0:T(8,128)} %param.34) | copy-start | bytes 98308
  214.9 12.9 %all-to-all-start.2 = ((f32[8,4,16,128]{3,2,1,0:T(8,128)}), f32[8,4,16,128]{3,2,1,0:T(8,128)S(1)}, u32[]{:S(2)}, u32[]{:S(2)}) async-start(f32[8,4,16,128]{3,2,1,0:T(8,128)} %get-tuple-element.85), calls=%async_computation.2 | async-start | bytes 524288 | tf_op jit(solution)/shard_map/all_to_all | solution.py:131
  218.3 100.2 %reduce-scatter.2.cloned.1.call-start = ((), (), s32[]{:S(2)}) async-start(), calls=%async_computation.5 | async-start | bytes 7864320 | tf_op jit(solution)/shard_map/reduce_scatter | solution.py:149
  222.8 1.1 copy-start.7
  223.9 23.8 %collective-permute-start = (f32[2,512]{1,0:T(2,128)S(1)}, f32[2,512]{1,0:T(2,128)S(1)}, u32[]{:S(2)}, u32[]{:S(2)}) collective-permute-start(f32[2,512]{1,0:T(2,128)S(1)} %slice.29), channel_id=1, source_target_pairs={{0,4},{4,8},{8,12},{12,16},{16,20},{20,24},{24,28},{1,5},{5,9},{9,... | collective-permute-start | bytes 12296 | tf_op jit(solution)/shard_map/ppermute | solution.py:19
  260.4 0.7 copy-start.6
  318.5 1.9 copy-start.1
Sparse Core Ops, SparseCore 0:
  8.9 31.2 all-gather.1
  260.6 57.9 reduce-scatter.1
where the time goes:
time: 330 us; the launch traced here: 328 us
  matrix products  127 us (38%)
  waiting for transfers between devices  97.7 us (30%)
  local copies, waits for them, and re-layouts  43.7 us (13%)
  other arithmetic  29.4 us (9%)
  starting transfers between devices  16.4 us (5%)
  between operations  13.6 us (4%)
    reduce_scatter x1, waiting for transfers between devices, shards(): lax.psum_scatter(jnp.dot(rec_out, recurrence_output_weight, preferred_ele...  57.4 us
    all_gather x1, waiting for transfers between devices, shards(): collected_rows = lax.all_gather(layer_input, 'tp', axis=1, tiled=True)  30 us
    dot_general x5, matrix products, shards(): jnp.dot(normed, weight, preferred_element_type=jnp.float32)  27.2 us
    dot_general x12, matrix products, block_pass(): jnp.einsum('bqy,byx->bqx', query_scaled_rows, latent_state, precision=PRE...  23.4 us
    dot_general x12, matrix products, block_pass(): jnp.einsum('otm,ote->ome', scaled_key * jnp.exp(block_total)[:, None, :],...  19.4 us
    dynamic_update_slice x12, other arithmetic, shards(): lax.scan(block_pass, (zero_state, zero_total), (to_blocks(query_rows, DK)...  19.2 us
    dot_general x12, matrix products, block_pass(): jnp.einsum('htk,hsk->hts', query_scaled_rows, scaled_key, precision=PRECI...  15.9 us
    dot_general x12, matrix products, block_pass(): jnp.einsum('hts,hsv->htv', scores, value_rows, precision=PRECISE_PRODUCT)  14 us
  transfers between devices with their start and end apart: 6, of which 4 were waited for; matrix products, arithmetic and copies ran while one was open for 10% of the time, Pallas kernels for 0%

commit v1 on v0

v1 whole, which is shorter than its diff:
```python
import functools

import jax
import jax.numpy as jnp
from jax import lax
from jax.experimental import pallas as pl
from jax.experimental.pallas import tpu as pltpu
from jax.sharding import PartitionSpec as P

DK = 128
DV = 128
CK = 3
EPS = 1e-06
F32 = jnp.float32
BF16 = jnp.bfloat16
ANY = pl.BlockSpec(memory_space=pl.ANY)
VMEM = pl.BlockSpec(memory_space=pltpu.VMEM)
SMEM = pl.BlockSpec(memory_space=pltpu.SMEM)


def xor_permute(value, axis, bit):
    peers = lax.axis_size(axis)
    return lax.ppermute(value, axis, [(i, i ^ bit) for i in range(peers)])


def from_behind(value, axis, by):
    peers = lax.axis_size(axis)
    return lax.ppermute(value, axis, [(i, i + by) for i in range(peers) if 0 <= i + by < peers])


def dot_nt(a, b):
    return lax.dot_general(a, b, (((1,), (1,)), ((), ())), preferred_element_type=F32)


def dot_tn(a, b):
    return lax.dot_general(a, b, (((0,), (0,)), ((), ())), preferred_element_type=F32)


def state_kernel(pieces, block, *refs):
    idx_ref = refs[0]
    xs = refs[1 : 1 + pieces]
    gain_ref, fm_ref, surge_ref, start_ref, wf_hbm, wv_hbm = refs[1 + pieces : 7 + pieces]
    normed_ref, v_ref, k_ref, c_ref, pre_ref, predecay_ref, pack_ref = refs[7 + pieces : 14 + pieces]
    wf, wv, sems = refs[14 + pieces :]
    copies = [
        pltpu.make_async_copy(wf_hbm, wf, sems.at[0]),
        pltpu.make_async_copy(wv_hbm, wv, sems.at[1]),
    ]
    for copy in copies:
        copy.start()
    tokens, width = xs[0].shape
    blocks = tokens // block
    heads = v_ref.shape[1] // DK
    step = block // 4

    def norm_rows(i, _):
        rows = pl.ds(pl.multiple_of(i * step, step), step)
        parts = [x[rows, :].astype(F32) for x in xs]
        total = sum(jnp.sum(part * part, axis=1, keepdims=True) for part in parts)
        scale = lax.rsqrt(total / (width * pieces) + EPS)
        for j, part in enumerate(parts):
            p = idx_ref[j]
            lanes = pl.ds(pl.multiple_of(p * width, 128), width)
            normed_ref[rows, lanes] = (part * scale * gain_ref[p].astype(F32)).astype(BF16)
        return 0

    lax.fori_loop(0, tokens // step, norm_rows, 0)
    for copy in copies:
        copy.wait()
    row = lax.broadcasted_iota(jnp.int32, (block, block), 0)
    col = lax.broadcasted_iota(jnp.int32, (block, block), 1)
    tri = jnp.where(row >= col, 1.0, 0.0).astype(BF16)
    room = 1.0 - fm_ref[...]
    pack_ref[...] = jnp.zeros(pack_ref.shape, BF16)
    pack_ref[:, DV : DV + start_ref.shape[1], :] = start_ref[...].astype(BF16)
    pre_ref[0] = jnp.zeros(pre_ref.shape[1:], F32)
    predecay_ref[0] = jnp.ones(predecay_ref.shape[1:], F32)

    def one_block(b, _):
        rows = pl.ds(pl.multiple_of(b * block, block), block)
        normed = normed_ref[rows, :]
        forget = jnp.dot(normed, wf[...], preferred_element_type=F32).astype(BF16).astype(F32)
        value = jnp.dot(normed, wv[...], preferred_element_type=F32).astype(BF16)
        v_ref[rows, :] = value
        keys = room * jax.nn.sigmoid(-forget)
        k_ref[rows, :] = keys
        log_forget = jnp.log1p(-keys) + surge_ref[rows, :]
        high = log_forget.astype(BF16)
        low = (log_forget - high.astype(F32)).astype(BF16)
        total = jnp.dot(tri, high, preferred_element_type=F32) + jnp.dot(
            tri, low, preferred_element_type=F32
        )
        c_ref[rows, :] = total
        end = total[block - 1 : block, :]
        scaled = (keys * jnp.exp(end - total)).astype(BF16)
        decay = jnp.exp(end)
        after_decay = predecay_ref[b] * decay
        predecay_ref[b + 1] = after_decay
        for h in range(heads):
            span = slice(h * DK, (h + 1) * DK)
            after = decay[:, span] * pre_ref[b, h] + dot_tn(value[:, span], scaled[:, span])
            pre_ref[b + 1, h] = after
        return 0

    lax.fori_loop(0, blocks, one_block, 0)
    last = predecay_ref[blocks]
    last_high = last.astype(BF16)
    last_low = (last - last_high.astype(F32)).astype(BF16)
    for h in range(heads):
        span = slice(h * DK, (h + 1) * DK)
        pack_ref[h, :DV, :] = pre_ref[blocks, h].astype(BF16)
        base = DV + start_ref.shape[1]
        pack_ref[h, base : base + 1, :] = last_high[:, span]
        pack_ref[h, base + 1 : base + 2, :] = last_low[:, span]


def conv_in_kernel(normed_ref, wa_hbm, wb_hbm, mixed_ref, wa, wb, sems):
    copies = [
        pltpu.make_async_copy(wa_hbm, wa, sems.at[0]),
        pltpu.make_async_copy(wb_hbm, wb, sems.at[1]),
    ]
    for copy in copies:
        copy.start()
    for copy in copies:
        copy.wait()
    step = 256

    def rows_of(i, _):
        rows = pl.ds(pl.multiple_of(i * step, step), step)
        normed = normed_ref[rows, :]
        first = jnp.dot(normed, wa[...], preferred_element_type=F32).astype(BF16).astype(F32)
        second = jnp.dot(normed, wb[...], preferred_element_type=F32).astype(BF16).astype(F32)
        mixed_ref[rows, :] = first * second
        return 0

    lax.fori_loop(0, normed_ref.shape[0] // step, rows_of, 0)


def project_kernel(count, *refs):
    normed_ref = refs[0]
    hbm = refs[1 : 1 + count]
    outs = refs[1 + count : 1 + 2 * count]
    bufs = refs[1 + 2 * count : 1 + 3 * count]
    sems = refs[1 + 3 * count]
    copies = [pltpu.make_async_copy(hbm[i], bufs[i], sems.at[i]) for i in range(count)]
    for copy in copies:
        copy.start()
    step = 256
    for i in range(count):
        copies[i].wait()

        def rows_of(r, _):
            rows = pl.ds(pl.multiple_of(r * step, step), step)
            outs[i][rows, :] = jnp.dot(
                normed_ref[rows, :], bufs[i][...], preferred_element_type=F32
            ).astype(BF16)
            return 0

        lax.fori_loop(0, normed_ref.shape[0] // step, rows_of, 0)


def mix_kernel(outputs, ids_ref, *refs):
    (
        q_ref, k_ref, c_ref, v_ref, og_ref, post_ref, mixed_ref, edge_ref, rim_ref, taps_ref,
        hgain_ref, enter_ref, pre_ref, predecay_ref, wr_ref, wc_ref,
    ) = refs[:16]
    outs = refs[16 : 16 + outputs]
    i = pl.program_id(0)
    b = ids_ref[i]
    block, width = q_ref.shape
    heads = width // DK
    sub = block // 4
    row = lax.broadcasted_iota(jnp.int32, (block, block), 0)
    col = lax.broadcasted_iota(jnp.int32, (block, block), 1)
    inner = (row // sub == col // sub) & (row >= col)
    near = (row // (2 * sub) == col // (2 * sub)) & (row // sub > col // sub)
    far = row // (2 * sub) > col // (2 * sub)
    rec = []
    for h in range(heads):
        span = slice(h * DK, (h + 1) * DK)
        q = q_ref[:, span].astype(F32)
        q = q * jax.nn.sigmoid(q) * (DK ** -0.5)
        k = k_ref[:, span]
        c = c_ref[:, span]
        v = v_ref[:, span]
        c4 = c.reshape(4, sub, DK)
        d4 = (c4 - c4[:, sub // 2 : sub // 2 + 1, :]).reshape(block, DK)
        c2 = c.reshape(2, 2 * sub, DK)
        d2 = (c2 - c2[:, sub - 1 : sub, :]).reshape(block, DK)
        d1 = c - c[2 * sub - 1 : 2 * sub, :]
        s4 = dot_nt((q * jnp.exp(d4)).astype(BF16), (k * jnp.exp(-d4)).astype(BF16))
        s2 = dot_nt(
            (q * jnp.exp(jnp.minimum(d2, 0.0))).astype(BF16),
            (k * jnp.exp(jnp.minimum(-d2, 0.0))).astype(BF16),
        )
        s1 = dot_nt(
            (q * jnp.exp(jnp.minimum(d1, 0.0))).astype(BF16),
            (k * jnp.exp(jnp.minimum(-d1, 0.0))).astype(BF16),
        )
        scores = jnp.where(inner, s4, jnp.where(near, s2, jnp.where(far, s1, 0.0)))
        state = pre_ref[0, h] + predecay_ref[0, :, span] * enter_ref[h]
        out = jnp.dot(scores.astype(BF16), v, preferred_element_type=F32) + dot_nt(
            (q * jnp.exp(c)).astype(BF16), state.astype(BF16)
        )
        scale = lax.rsqrt(jnp.mean(out * out, axis=1, keepdims=True) + EPS)
        gate = og_ref[:, span].astype(F32)
        gate = gate * jax.nn.sigmoid(gate)
        rec.append((out * scale * hgain_ref[...].astype(F32) * gate).astype(BF16))
    rec = jnp.concatenate(rec, axis=1)
    mixed = mixed_ref[...]
    edge = jnp.where(b == 0, rim_ref[...], edge_ref[...])
    padded = jnp.concatenate([edge, mixed], axis=0)
    taps = taps_ref[...].astype(F32)
    base = edge.shape[0] - (CK - 1)
    conv = padded[base : base + block] * taps[0:1]
    for j in range(1, CK):
        conv = conv + padded[base + j : base + j + block] * taps[j : j + 1]
    conv = (post_ref[...].astype(F32) * conv).astype(BF16)
    result = (
        jnp.dot(rec, wr_ref[...], preferred_element_type=F32)
        + jnp.dot(conv, wc_ref[...], preferred_element_type=F32)
    ).astype(BF16)
    for n in range(outputs):

        @pl.when(i == n)
        def _():
            outs[n][...] = result


def shards(
    layer_input,
    input_norm_gain,
    query_weight,
    forget_weight,
    value_matrix,
    output_gate_weight,
    after_gate_weight,
    before_gate_weight,
    convolution_input_weight,
    forget_minimum,
    surge_log_decay,
    convolution_kernel,
    head_norm_gain,
    starting_state,
    recurrence_output_weight,
    convolution_output_weight,
    output_norm_gain,
):
    tokens, piece = layer_input.shape
    features, width = query_weight.shape
    heads = width // DK
    tp = lax.axis_size("tp")
    sp = lax.axis_size("sp")
    me = lax.axis_index("tp")
    at = lax.axis_index("sp")
    block = tokens // tp
    blocks = tp

    held = [layer_input]
    order = [0]
    bit = tp // 2
    while bit:
        held = held + [xor_permute(x, "tp", bit) for x in held]
        order = order + [m | bit for m in order]
        bit //= 2
    ids = jnp.stack([me ^ m for m in order]).astype(jnp.int32)

    sds = jax.ShapeDtypeStruct
    krows = starting_state.shape[1]
    pack_rows = DV + krows + 16
    params = pltpu.CompilerParams(vmem_limit_bytes=56 * 1024 * 1024)
    weight_buf = pltpu.VMEM((features, width), BF16)
    normed, value, keys, decay, pre, predecay, pack = pl.pallas_call(
        functools.partial(state_kernel, tp, block),
        out_shape=(
            sds((tokens, features), BF16),
            sds((tokens, width), BF16),
            sds((tokens, width), F32),
            sds((tokens, width), F32),
            sds((blocks + 1, heads, DV, DK), F32),
            sds((blocks + 1, 1, width), F32),
            sds((heads, pack_rows, 128), BF16),
        ),
        in_specs=[SMEM] + [VMEM] * tp + [VMEM] * 4 + [ANY] * 2,
        out_specs=[VMEM] * 7,
        scratch_shapes=[weight_buf, weight_buf, pltpu.SemaphoreType.DMA((2,))],
        compiler_params=params,
        name="state",
    )(
        ids,
        *held,
        input_norm_gain.reshape(tp, 1, piece),
        forget_minimum.reshape(1, width),
        surge_log_decay,
        starting_state,
        forget_weight,
        value_matrix,
    )

    every = lax.all_gather(pack, "sp", axis=0, tiled=False)

    mixed_in = pl.pallas_call(
        conv_in_kernel,
        out_shape=sds((tokens, width), F32),
        in_specs=[VMEM, ANY, ANY],
        out_specs=VMEM,
        scratch_shapes=[weight_buf, weight_buf, pltpu.SemaphoreType.DMA((2,))],
        compiler_params=params,
        name="conv_in",
    )(normed, before_gate_weight, convolution_input_weight)
    rim = from_behind(mixed_in[tokens - 8 :], "sp", 1)
    query, outgate, postgate = pl.pallas_call(
        functools.partial(project_kernel, 3),
        out_shape=[sds((tokens, width), BF16)] * 3,
        in_specs=[VMEM] + [ANY] * 3,
        out_specs=[VMEM] * 3,
        scratch_shapes=[weight_buf] * 3 + [pltpu.SemaphoreType.DMA((3,))],
        compiler_params=params,
        name="project",
    )(normed, query_weight, output_gate_weight, after_gate_weight)

    states = every[:, :, :DV, :].astype(F32)
    totals = jnp.sum(every[:, :, DV + krows : DV + krows + 2, :].astype(F32), axis=2, keepdims=True)
    start = every[:, :, DV : DV + krows, :].astype(F32)
    enter = start.transpose(1, 3, 0, 2).reshape(heads, DV, DK)
    for j in range(sp - 1):
        enter = jnp.where(j < at, totals[j] * enter + states[j], enter)

    half = tp // 2
    rows8 = block // 8

    def mix(block_ids):
        count = len(block_ids)
        at_block = lambda i, ids: (ids[i], 0)
        whole = lambda *shape: pl.BlockSpec(shape, lambda i, ids: (0,) * len(shape))
        tile = pl.BlockSpec((block, width), at_block)
        return pl.pallas_call(
            functools.partial(mix_kernel, count),
            grid_spec=pltpu.PrefetchScalarGridSpec(
                num_scalar_prefetch=1,
                grid=(count,),
                in_specs=[
                    tile, tile, tile, tile, tile, tile, tile,
                    pl.BlockSpec((8, width), lambda i, ids: (jnp.maximum(ids[i] * rows8 - 1, 0), 0)),
                    whole(8, width),
                    whole(CK, width),
                    whole(1, DV),
                    whole(heads, DV, DK),
                    pl.BlockSpec((1, heads, DV, DK), lambda i, ids: (ids[i], 0, 0, 0)),
                    pl.BlockSpec((1, 1, width), lambda i, ids: (ids[i], 0, 0)),
                    whole(width, features),
                    whole(width, features),
                ],
                out_specs=[whole(block, features)] * count,
            ),
            out_shape=[sds((block, features), BF16)] * count,
            compiler_params=params,
            name="mix",
        )(
            jnp.stack(block_ids).astype(jnp.int32),
            query, keys, decay, value, outgate, postgate, mixed_in, mixed_in, rim,
            convolution_kernel, head_norm_gain.reshape(1, DV), enter, pre, predecay,
            recurrence_output_weight, convolution_output_weight,
        )

    def fold(parts):
        parts = list(parts)
        step = len(parts) // 2
        bit = 1
        while step:
            moved = [xor_permute(parts[m], "tp", bit) for m in range(1, len(parts), 2)]
            parts = [
                (parts[2 * n].astype(F32) + moved[n].astype(F32)).astype(BF16)
                for n in range(step)
            ]
            step //= 2
            bit *= 2
        return parts[0]

    away = fold(mix([me ^ (half + m) for m in range(half)]))
    arrived = xor_permute(away, "tp", half)
    home = fold(mix([me ^ m for m in range(half)]))
    mixed = home.astype(F32) + arrived.astype(F32)
    scale = lax.rsqrt(jnp.mean(mixed * mixed, axis=-1, keepdims=True) + EPS)
    return (mixed * scale * output_norm_gain.astype(F32)).astype(BF16)


def solution(mesh):
    return jax.shard_map(
        shards,
        mesh=mesh,
        in_specs=(
            P("sp", "tp"),
            P(),
            P(None, "tp"),
            P(None, "tp"),
            P(None, "tp"),
            P(None, "tp"),
            P(None, "tp"),
            P(None, "tp"),
            P(None, "tp"),
            P("tp"),
            P("sp", "tp"),
            P(None, "tp"),
            P(),
            P("tp", "sp", None),
            P("tp", None),
            P("tp", None),
            P(),
        ),
        out_specs=P(("sp", "tp"), None),
        check_vma=False,
    )
```

time: 330 us -> 142 us (0.43)
  matrix products: 127 us -> 0 us
  Pallas kernels: 0 us -> 52.3 us
  waiting for transfers between devices: 97.7 us -> 54.7 us
  local copies, waits for them, and re-layouts: 43.7 us -> 3.71 us
  other arithmetic: 29.4 us -> 8.13 us
  starting transfers between devices: 16.4 us -> 8.79 us
    dot_general x56 -> x0, matrix products: 127 us -> none  [the longest x5 27.2 us: shards(): jnp.dot(normed, weight, preferred_element_type=jnp.float32)]
    reduce_scatter x1 -> x0, waiting for transfers between devices: 57.4 us -> none  [shards(): lax.psum_scatter(jnp.dot(rec_out, recurrence_output_weight, preferred_ele...]
    pallas_call x0 -> x5, Pallas kernels: none -> 52.3 us  [the longest x2 18.9 us: mix(): pl.pallas_call(functools.partial(mix_kernel, count), grid_spec=pltpu.Pref...]
    ppermute x1 -> x7, waiting for transfers between devices: 0.01 us -> 36.1 us  [the longest x6 36.1 us: xor_permute(): return lax.ppermute(value, axis, [(i, i ^ bit) for i in range(peers)])]
    dynamic_update_slice x12 -> x0, other arithmetic: 19.2 us -> none  [shards(): lax.scan(block_pass, (zero_state, zero_total), (to_blocks(query_rows, DK)...]
    transpose x4 -> x0, local copies, waits for them, and re-layouts: 12.7 us -> none  [the longest x3 9.04 us: to_blocks(): value_rows.reshape(blocks, BLK, heads_local, width).transpose(0, 2, 1, 3)]
    all_to_all x3 -> x0, starting transfers between devices: 12.5 us -> none  [the longest x1 5.52 us: shards(): lax.all_to_all(local_total[None, :, :, None], 'sp', split_axis=2, concat_...]
    all_gather x1, waiting for transfers between devices: 30 us -> 18.6 us  [shards(): every = lax.all_gather(pack, 'sp', axis=0, tiled=False)]
  transfers between devices with their start and end apart: 6 -> 8, of which waited for: 4 -> 5; matrix products, arithmetic and copies ran while one was open for 10% -> 6% of each run, Pallas kernels for 0% -> 21%
where the time goes in v1:
time: 142 us; the launch traced here: 141 us
  waiting for transfers between devices  54.7 us (39%)
  Pallas kernels  52.3 us (37%)
  between operations  13.5 us (10%)
  starting transfers between devices  8.79 us (6%)
  other arithmetic  8.13 us (6%)
  local copies, waits for them, and re-layouts  3.71 us (3%)
    ppermute x6, waiting for transfers between devices, xor_permute(): return lax.ppermute(value, axis, [(i, i ^ bit) for i in range(peers)])  36.1 us
    pallas_call x2, Pallas kernels, mix(): pl.pallas_call(functools.partial(mix_kernel, count), grid_spec=pltpu.Pref...  18.9 us
    all_gather x1, waiting for transfers between devices, shards(): every = lax.all_gather(pack, 'sp', axis=0, tiled=False)  18.6 us
    pallas_call x1, Pallas kernels, shards(): pl.pallas_call(functools.partial(state_kernel, tp, block), out_shape=(sds...  13.5 us
    pallas_call x1, Pallas kernels, shards(): pl.pallas_call(functools.partial(project_kernel, 3), out_shape=[sds((toke...  10.8 us
    pallas_call x1, Pallas kernels, shards(): pl.pallas_call(conv_in_kernel, out_shape=sds((tokens, width), F32), in_sp...  9.03 us
    ppermute x6, starting transfers between devices, xor_permute(): return lax.ppermute(value, axis, [(i, i ^ bit) for i in range(peers)])  5.13 us
    ppermute x1, starting transfers between devices, from_behind(): lax.ppermute(value, axis, [(i, i + by) for i in range(peers) if 0 <= i +...  3.66 us
  transfers between devices with their start and end apart: 8, of which 5 were waited for; matrix products, arithmetic and copies ran while one was open for 6% of the time, Pallas kernels for 21%

profile of v1, /device:TPU:0, one launch (start us, length us, event | category | flops | bytes accessed | tf_op | source)
XLA Modules:
  0.0 141.1 jit_solution(11825138380078649178)
XLA Ops:
  6.5 0.0 all-gather.3.cloned.1.call-start
  6.5 3.0 %collective-permute-start = (bf16[768,512]{1,0:T(8,128)(2,1)}, bf16[768,512]{1,0:T(8,128)(2,1)S(1)}, u32[]{:S(2)}, u32[]{:S(2)}) collective-permute-start(bf16[768,512]{1,0:T(8,128)(2,1)} %refs_1_.2), channel_id=1, source_target_pairs={{0,2},{1,3},{2,0},{3,1},{4,6},{5,7},{6,4},{7,5},{8,10},{9,11},{10,... | collective-permute-start | bytes 2359304 | tf_op jit(solution)/shard_map/ppermute | solution.py:23
  9.5 0.0 collective-permute-start.1
  9.5 17.7 %collective-permute-done.refs_2_ = bf16[768,512]{1,0:T(8,128)(2,1)S(1)} collective-permute-done((bf16[768,512]{1,0:T(8,128)(2,1)}, bf16[768,512]{1,0:T(8,128)(2,1)S(1)}, u32[]{:S(2)}, u32[]{:S(2)}) %collective-permute-start) | collective-permute-done | bytes 786464 | tf_op jit(solution)/shard_map/ppermute | solution.py:23
  27.3 0.0 copy-start.1
  27.3 0.0 collective-permute-start.2
  27.3 1.3 reshape.55.refs_5_
  28.6 0.6 pad_add_fusion.1.refs_0_
  29.2 0.0 collective-permute-done.1.refs_3_
  29.2 0.0 copy-start.2
  29.2 0.4 collective-permute-done.2.refs_4_
  29.5 0.0 copy-start.3
  29.5 0.0 copy-done.1
  29.5 0.5 copy-done.2
  30.1 0.4 copy-done.3
  30.4 13.5 %state.1 = (bf16[768,2048]{1,0:T(8,128)(2,1)}, bf16[768,512]{1,0:T(8,128)(2,1)}, f32[768,512]{1,0:T(8,128)}, f32[768,512]{1,0:T(8,128)}, f32[5,4,128,128]{3,2,1,...) custom-call(s32[4]{0:T(128)} %pad_add_fusion.1.refs_0_, bf16[768,512]{1,0:T(8,128)(2,1)} %refs_1_.2, ...), custom_call_target="tpu_custom_call" | custom-call | tf_op jit(solution)/shard_map/state/pallas_call | solution.py:273
  44.0 0.0 all-gather.3.cloned.1.call-update
  44.0 0.7 pad_add_fusion.2.ids_ref
  44.7 9.0 %conv_in.1.refs_6_.refs_7_ = f32[768,512]{1,0:T(8,128)} custom-call(bf16[768,2048]{1,0:T(8,128)(2,1)} %get-tuple-element.19.refs_0_.normed_ref, bf16[2048,512]{1,0:T(8,128)(2,1)} %wa_hbm.1, bf16[2048,512]{1,0:T(8,128)(2,1)} %wb_hbm.1), custom_call_target="tpu_custom_call" | custom-call | tf_op jit(solution)/shard_map/conv_in/pallas_call | solution.py:302
  53.7 0.7 slice.79
  54.4 3.7 %collective-permute-start.3 = (f32[8,512]{1,0:T(8,128)S(1)}, f32[8,512]{1,0:T(8,128)S(1)}, u32[]{:S(2)}, u32[]{:S(2)}) collective-permute-start(f32[8,512]{1,0:T(8,128)S(1)} %slice.79), channel_id=1, source_target_pairs={{0,4},{4,8},{8,12},{12,16},{16,20},{20,24},{24,28},{1,5},{5,9},{9,... | collective-permute-start | bytes 49160 | tf_op jit(solution)/shard_map/ppermute | solution.py:28
  58.1 10.8 %project.1 = (bf16[768,512]{1,0:T(8,128)(2,1)}, bf16[768,512]{1,0:T(8,128)(2,1)}, bf16[768,512]{1,0:T(8,128)(2,1)}) custom-call(bf16[768,2048]{1,0:T(8,128)(2,1)} %get-tuple-element.19.refs_0_.normed_ref, bf16[2048,512]{1,0:T(8,128)(2,1)} %refs_1_.3, bf16[2048,512]{1,0:T(8,128)(2,1)} %refs_2_.1, bf16[2048,512]{1,0:T(8,128)(2,1)} %refs_3_.1), custom_call_target="tpu_custom_call" | custom-call | tf_op jit(solution)/shard_map/project/pallas_call | solution.py:312
  68.9 18.6 %all-gather.3.cloned.1.call-done = bf16[32,160,128]{2,1,0:T(8,128)(2,1)} async-done(((bf16[4,160,128]{2,1,0:T(8,128)(2,1)}), bf16[32,160,128]{2,1,0:T(8,128)(2,1)}) %all-gather.3.cloned.1.call-update) | async-done | bytes 1310736 | tf_op jit(solution)/shard_map/all_gather | solution.py:300
  87.5 0.9 convert_reduce_fusion
  88.4 1.5 %slice_convert_fusion = f32[8,4,128,128]{3,2,1,0:T(8,128)S(1)} fusion(bf16[8,4,160,128]{3,2,1,0:T(8,128)(2,1)} %bitcast.79), kind=kLoop, calls=%fused_computation.5 | loop fusion | flops 524288 | bytes 3145728 | tf_op jit(solution)/shard_map/convert_element_type | solution.py:322
  89.8 0.9 convert_bitcast_fusion
  90.8 0.1 copy.25
  91.0 0.9 fusion.1.refs_11_
  91.9 0.0 collective-permute-done.3.refs_8_
  91.9 0.0 copy-start.5
  91.9 0.6 copy-done.5
  92.5 9.4 %mix.3 = (bf16[192,2048]{1,0:T(8,128)(2,1)}, bf16[192,2048]{1,0:T(8,128)(2,1)}) custom-call(s32[2]{0:T(128)} %pad_add_fusion.2.ids_ref, bf16[768,512]{1,0:T(8,128)(2,1)} %get-tuple-element.20.refs_0_, f32[768,512]{1,0:T(8,128)} %get-tuple-element.21.refs_1_, f32[768,512]{1,0:T(8,128)} %get-tuple-element.22.refs_2_, ...), custom_call_target="tpu_custom_call" | custom-call | tf_op jit(solution)/shard_map/mix/pallas_call | solution.py:337
  101.9 0.1 collective-permute-start.5
  101.9 0.6 pad_add_fusion.ids_ref
  102.5 9.5 %mix.2 = (bf16[192,2048]{1,0:T(8,128)(2,1)}, bf16[192,2048]{1,0:T(8,128)(2,1)}) custom-call(s32[2]{0:T(128)} %pad_add_fusion.ids_ref, bf16[768,512]{1,0:T(8,128)(2,1)} %get-tuple-element.20.refs_0_, f32[768,512]{1,0:T(8,128)} %get-tuple-element.21.refs_1_, f32[768,512]{1,0:T(8,128)} %get-tuple-element.22.refs_2_, ...), custom_call_target="tpu_custom_call" | custom-call | tf_op jit(solution)/shard_map/mix/pallas_call | solution.py:337
  112.1 0.0 copy-start.6
  112.1 0.0 copy-start
  112.1 0.6 collective-permute-start.4
  112.7 0.0 collective-permute-done.5
  112.7 0.0 copy-done.4
  112.7 0.3 add_convert_fusion
  112.9 1.5 %collective-permute-start.6 = (bf16[192,2048]{1,0:T(8,128)(2,1)S(1)}, bf16[192,2048]{1,0:T(8,128)(2,1)S(1)}, u32[]{:S(2)}, u32[]{:S(2)}) collective-permute-start(bf16[192,2048]{1,0:T(8,128)(2,1)S(1)} %add_convert_fusion), channel_id=1, source_target_pairs={{0,2},{1,3},{2,0},{3,1},{4,6},{5,7},{6,4},{7,5},{8,10},{9,11},{10,... | collective-permute-start | bytes 2359304 | tf_op jit(solution)/shard_map/ppermute | solution.py:23
  114.5 0.0 copy-done.6
  114.5 0.3 collective-permute-done.4
  114.8 17.7 %collective-permute-done.6 = bf16[192,2048]{1,0:T(8,128)(2,1)S(1)} collective-permute-done((bf16[192,2048]{1,0:T(8,128)(2,1)S(1)}, bf16[192,2048]{1,0:T(8,128)(2,1)S(1)}, u32[]{:S(2)}, u32[]{:S(2)}) %collective-permute-start.6) | collective-permute-done | bytes 786464 | tf_op jit(solution)/shard_map/ppermute | solution.py:23
  132.5 0.0 copy-done
  132.5 0.4 multiply_reduce_fusion
  132.9 1.4 multiply_convert_fusion
  (5 shorter events, 0.0 us)
Async XLA Ops:
  6.5 81.0 %all-gather.3.cloned.1.call-start = ((), (), s32[]{:S(2)}) async-start(), calls=%async_computation | async-start | bytes 1474560 | tf_op jit(solution)/shard_map/all_gather | solution.py:300
  6.5 20.7 %collective-permute-start = (bf16[768,512]{1,0:T(8,128)(2,1)}, bf16[768,512]{1,0:T(8,128)(2,1)S(1)}, u32[]{:S(2)}, u32[]{:S(2)}) collective-permute-start(bf16[768,512]{1,0:T(8,128)(2,1)} %refs_1_.2), channel_id=1, source_target_pairs={{0,2},{1,3},{2,0},{3,1},{4,6},{5,7},{6,4},{7,5},{8,10},{9,11},{10,... | collective-permute-start | bytes 2359304 | tf_op jit(solution)/shard_map/ppermute | solution.py:23
  9.5 19.7 %collective-permute-start.1 = (bf16[768,512]{1,0:T(8,128)(2,1)}, bf16[768,512]{1,0:T(8,128)(2,1)S(1)}, u32[]{:S(2)}, u32[]{:S(2)}) collective-permute-start(bf16[768,512]{1,0:T(8,128)(2,1)} %refs_1_.2), channel_id=1, source_target_pairs={{0,1},{1,0},{2,3},{3,2},{4,5},{5,4},{6,7},{7,6},{8,9},{9,8},{10,11... | collective-permute-start | bytes 2359304 | tf_op jit(solution)/shard_map/ppermute | solution.py:23
  27.3 2.3 %copy-start.1 = (bf16[768,512]{1,0:T(8,128)(2,1)}, bf16[768,512]{1,0:T(8,128)(2,1)S(1)}, u32[]{:S(2)}) copy-start(bf16[768,512]{1,0:T(8,128)(2,1)S(1)} %collective-permute-done.refs_2_) | copy-start | bytes 2359300
  27.3 2.3 %collective-permute-start.2 = (bf16[768,512]{1,0:T(8,128)(2,1)S(1)}, bf16[768,512]{1,0:T(8,128)(2,1)S(1)}, u32[]{:S(2)}, u32[]{:S(2)}) collective-permute-start(bf16[768,512]{1,0:T(8,128)(2,1)S(1)} %collective-permute-done.refs_2_), channel_id=1, source_target_pairs={{0,1},{1,0},{2,3},{3,2},{4,5},{5,4},{6,7},{7,6},{8,9},{9,8},{10,11... | collective-permute-start | bytes 2359304 | tf_op jit(solution)/shard_map/ppermute | solution.py:23
  29.2 0.9 copy-start.2
  29.5 0.9 copy-start.3
  54.4 37.5 %collective-permute-start.3 = (f32[8,512]{1,0:T(8,128)S(1)}, f32[8,512]{1,0:T(8,128)S(1)}, u32[]{:S(2)}, u32[]{:S(2)}) collective-permute-start(f32[8,512]{1,0:T(8,128)S(1)} %slice.79), channel_id=1, source_target_pairs={{0,4},{4,8},{8,12},{12,16},{16,20},{20,24},{24,28},{1,5},{5,9},{9,... | collective-permute-start | bytes 49160 | tf_op jit(solution)/shard_map/ppermute | solution.py:28
  91.9 0.6 copy-start.5
  101.9 10.8 %collective-permute-start.5 = (bf16[192,2048]{1,0:T(8,128)(2,1)}, bf16[192,2048]{1,0:T(8,128)(2,1)S(1)}, u32[]{:S(2)}, u32[]{:S(2)}) collective-permute-start(bf16[192,2048]{1,0:T(8,128)(2,1)} %get-tuple-element.32), channel_id=1, source_target_pairs={{0,1},{1,0},{2,3},{3,2},{4,5},{5,4},{6,7},{7,6},{8,9},{9,8},{10,11... | collective-permute-start | bytes 2359304 | tf_op jit(solution)/shard_map/ppermute | solution.py:23
  102.5 10.1 %copy-start.4 = (bf16[192,2048]{1,0:T(8,128)(2,1)S(1)}, bf16[192,2048]{1,0:T(8,128)(2,1)}, u32[]{:S(2)}) copy-start(bf16[192,2048]{1,0:T(8,128)(2,1)} %get-tuple-element.31) | copy-start | bytes 2359300
  112.1 2.4 %copy-start.6 = (bf16[2048]{0:T(1024)(128)(2,1)S(1)}, bf16[2048]{0:T(1024)(128)(2,1)}, u32[]{:S(2)}) copy-start(bf16[2048]{0:T(1024)(128)(2,1)} %param.33) | copy-start | bytes 12292
  112.1 20.4 %copy-start = (bf16[192,2048]{1,0:T(8,128)(2,1)S(1)}, bf16[192,2048]{1,0:T(8,128)(2,1)}, u32[]{:S(2)}) copy-start(bf16[192,2048]{1,0:T(8,128)(2,1)} %get-tuple-element.29) | copy-start | bytes 2359300
  112.1 2.7 %collective-permute-start.4 = (bf16[192,2048]{1,0:T(8,128)(2,1)}, bf16[192,2048]{1,0:T(8,128)(2,1)S(1)}, u32[]{:S(2)}, u32[]{:S(2)}) collective-permute-start(bf16[192,2048]{1,0:T(8,128)(2,1)} %get-tuple-element.30), channel_id=1, source_target_pairs={{0,1},{1,0},{2,3},{3,2},{4,5},{5,4},{6,7},{7,6},{8,9},{9,8},{10,11... | collective-permute-start | bytes 2359304 | tf_op jit(solution)/shard_map/ppermute | solution.py:23
  112.9 19.5 %collective-permute-start.6 = (bf16[192,2048]{1,0:T(8,128)(2,1)S(1)}, bf16[192,2048]{1,0:T(8,128)(2,1)S(1)}, u32[]{:S(2)}, u32[]{:S(2)}) collective-permute-start(bf16[192,2048]{1,0:T(8,128)(2,1)S(1)} %add_convert_fusion), channel_id=1, source_target_pairs={{0,2},{1,3},{2,0},{3,1},{4,6},{5,7},{6,4},{7,5},{8,10},{9,11},{10,... | collective-permute-start | bytes 2359304 | tf_op jit(solution)/shard_map/ppermute | solution.py:23
Sparse Core Ops, SparseCore 0:
  44.1 43.3 all-gather.2

commit v2 on v1

v2 whole, which is shorter than its diff:
```python
import functools

import jax
import jax.numpy as jnp
from jax import lax
from jax.experimental import pallas as pl
from jax.experimental.pallas import tpu as pltpu
from jax.sharding import PartitionSpec as P

DK = 128
DV = 128
CK = 3
EPS = 1e-06
F32 = jnp.float32
BF16 = jnp.bfloat16
ANY = pl.BlockSpec(memory_space=pl.ANY)
SMEM = pl.BlockSpec(memory_space=pltpu.SMEM)


def xor_permute(value, axis, bit):
    peers = lax.axis_size(axis)
    return lax.ppermute(value, axis, [(i, i ^ bit) for i in range(peers)])


def dot_nt(a, b):
    return lax.dot_general(a, b, (((1,), (1,)), ((), ())), preferred_element_type=F32)


def dot_tn(a, b):
    return lax.dot_general(a, b, (((0,), (0,)), ((), ())), preferred_element_type=F32)


class Refs:
    def __init__(self, names, refs):
        self.__dict__.update(zip(names, refs))

    def get(self, name):
        return self.__dict__[name]


def named_call(body, name, ins, outs, scratch, aliases=None):
    names = list(ins) + list(outs) + list(scratch)
    in_names, out_names = list(ins), list(outs)
    aliases = aliases or {}

    def kernel(*refs):
        body(Refs(names, refs))

    results = pl.pallas_call(
        kernel,
        grid=(1,),
        out_shape=[shape for shape, _ in outs.values()],
        in_specs=[spec for _, spec in ins.values()],
        out_specs=[spec for _, spec in outs.values()],
        scratch_shapes=list(scratch.values()),
        input_output_aliases={in_names.index(a): out_names.index(b) for a, b in aliases.items()},
        compiler_params=pltpu.CompilerParams(vmem_limit_bytes=56 * 1024 * 1024),
        name=name,
    )(*[array for array, _ in ins.values()])
    return dict(zip(out_names, results))


def weight_copies(r, weights):
    copies = {}
    for n, w in enumerate(weights):
        copies[w] = pltpu.make_async_copy(r.get("hbm_" + w), r.get("buf_" + w), r.sems.at[n])
        copies[w].start()
    return copies


def norm_piece(r, pieces):
    xs = [r.get("x%d" % j) for j in range(pieces)]
    tokens, width = xs[0].shape
    step = 48

    def norm_rows(i, _):
        rows = pl.ds(pl.multiple_of(i * step, step), step)
        parts = [x[rows, :].astype(F32) for x in xs]
        total = sum(jnp.sum(part * part, axis=1, keepdims=True) for part in parts)
        scale = lax.rsqrt(total / (width * pieces) + EPS)
        for j, part in enumerate(parts):
            p = r.ids[j]
            lanes = pl.ds(pl.multiple_of(p * width, 128), width)
            r.normed[rows, lanes] = (part * scale * r.gain[p].astype(F32)).astype(BF16)
        return 0

    lax.fori_loop(0, tokens // step, norm_rows, 0, unroll=2)


def project(r, copies, w):
    copies[w].wait()
    return jnp.dot(r.normed[...], r.get("buf_" + w)[...], preferred_element_type=F32).astype(BF16)


def forget_value_state(r, copies, block, first, last):
    r.forget[...] = project(r, copies, "forget")
    r.value[...] = project(r, copies, "value")
    tokens, width = r.value.shape
    heads = width // DK
    row = lax.broadcasted_iota(jnp.int32, (block, block), 0)
    col = lax.broadcasted_iota(jnp.int32, (block, block), 1)
    tri = jnp.where(row >= col, 1.0, 0.0).astype(BF16)
    for b in range(tokens // block):
        rows = slice(b * block, (b + 1) * block)
        for h in range(heads):
            span = slice(h * DK, (h + 1) * DK)
            keys = (1.0 - r.minimum[:, span]) * jax.nn.sigmoid(-r.forget[rows, span].astype(F32))
            r.keys[rows, span] = keys
            log_forget = jnp.log1p(-keys) + r.surge[rows, span]
            high = log_forget.astype(BF16)
            low = (log_forget - high.astype(F32)).astype(BF16)
            total = jnp.dot(tri, high, preferred_element_type=F32) + jnp.dot(
                tri, low, preferred_element_type=F32
            )
            r.decay[rows, span] = total
            end = total[block - 1 : block, :]
            scaled = (keys * jnp.exp(end - total)).astype(BF16)
            fade = jnp.exp(end)
            if b == 0 and first:
                before, sofar = jnp.zeros((DV, DK), F32), jnp.ones((1, DK), F32)
            elif b == 0:
                before, sofar = r.carry[h], r.carry_decay[:, span]
            else:
                before, sofar = r.pre[b, h], r.predecay[b, :, span]
            if b == 0:
                r.pre[0, h] = before
                r.predecay[0, :, span] = sofar
            after = fade * before + dot_tn(r.value[rows, span], scaled)
            sofar = sofar * fade
            if (b + 1) * block < tokens:
                r.pre[b + 1, h] = after
                r.predecay[b + 1, :, span] = sofar
            elif not last:
                r.carry_out[h] = after
                r.carry_decay_out[:, span] = sofar
            else:
                peers, _, rows_each, _ = r.pack.shape
                after = after.astype(BF16)
                high = sofar.astype(BF16)
                low = (sofar - high.astype(F32)).astype(BF16)
                for s in range(peers):
                    r.pack[s, h] = after[s * rows_each : (s + 1) * rows_each, :]
                    for part, line in ((high, h), (low, heads + h)):
                        at_row = line % rows_each
                        r.pack[s, heads + line // rows_each, at_row : at_row + 1, :] = part


def advance_kernel(r, heads):
    peers, _, rows_each, _ = r.moved.shape
    for h in range(heads):
        running = r.start[h]
        for s in range(peers):
            r.enter[s, h] = running.astype(BF16)
            total = sum(
                r.moved[s, heads + line // rows_each, line % rows_each : line % rows_each + 1, :].astype(F32)
                for line in (h, heads + h)
            )
            running = total * running + r.moved[s, h].astype(F32)
    edge = r.mixed[r.mixed.shape[0] - (CK - 1) :, :]
    lines = []
    for h in range(edge.shape[1] // DK):
        part = edge[:, h * DK : (h + 1) * DK]
        high = part.astype(BF16).astype(F32)
        lines += [high, part - high]
    lines = jnp.concatenate(lines, axis=0).astype(BF16)
    for n in range(lines.shape[0] // rows_each):
        for s in range(peers):
            r.enter[s, heads + n] = lines[n * rows_each : (n + 1) * rows_each, :]


def mix_kernel(outputs, ids_ref, *refs):
    (
        q_ref, k_ref, c_ref, v_ref, og_ref, post_ref, mixed_ref, edge_ref, taps_ref,
        hgain_ref, enter_ref, pre_ref, predecay_ref, wr_hbm, wc_hbm,
    ) = refs[:15]
    outs = refs[15 : 15 + outputs]
    wr_ref, wc_ref, sems = refs[15 + outputs :]
    i = pl.program_id(0)
    b = ids_ref[i]
    at = ids_ref[outputs]
    copies = [
        pltpu.make_async_copy(wr_hbm, wr_ref, sems.at[0]),
        pltpu.make_async_copy(wc_hbm, wc_ref, sems.at[1]),
    ]

    @pl.when(i == 0)
    def _():
        for copy in copies:
            copy.start()

    block, width = q_ref.shape
    heads = width // DK
    sub = block // 4
    row = lax.broadcasted_iota(jnp.int32, (block, block), 0)
    col = lax.broadcasted_iota(jnp.int32, (block, block), 1)
    inner = (row // sub == col // sub) & (row >= col)
    near = (row // (2 * sub) == col // (2 * sub)) & (row // sub > col // sub)
    far = row // (2 * sub) > col // (2 * sub)
    rec = []
    for h in range(heads):
        span = slice(h * DK, (h + 1) * DK)
        q = q_ref[:, span].astype(F32)
        q = q * jax.nn.sigmoid(q) * (DK ** -0.5)
        k = k_ref[:, span]
        c = c_ref[:, span]
        v = v_ref[:, span]
        c4 = c.reshape(4, sub, DK)
        d4 = (c4 - c4[:, sub // 2 : sub // 2 + 1, :]).reshape(block, DK)
        c2 = c.reshape(2, 2 * sub, DK)
        d2 = (c2 - c2[:, sub - 1 : sub, :]).reshape(block, DK)
        d1 = c - c[2 * sub - 1 : 2 * sub, :]
        s4 = dot_nt((q * jnp.exp(d4)).astype(BF16), (k * jnp.exp(-d4)).astype(BF16))
        s2 = dot_nt(
            (q * jnp.exp(jnp.minimum(d2, 0.0))).astype(BF16),
            (k * jnp.exp(jnp.minimum(-d2, 0.0))).astype(BF16),
        )
        s1 = dot_nt(
            (q * jnp.exp(jnp.minimum(d1, 0.0))).astype(BF16),
            (k * jnp.exp(jnp.minimum(-d1, 0.0))).astype(BF16),
        )
        scores = jnp.where(inner, s4, jnp.where(near, s2, jnp.where(far, s1, 0.0)))
        enter = jnp.concatenate(
            [enter_ref[s, h].astype(F32) for s in range(enter_ref.shape[0])], axis=0
        )
        state = pre_ref[0, h] + predecay_ref[0, :, span] * enter
        out = jnp.dot(scores.astype(BF16), v, preferred_element_type=F32) + dot_nt(
            (q * jnp.exp(c)).astype(BF16), state.astype(BF16)
        )
        scale = lax.rsqrt(jnp.mean(out * out, axis=1, keepdims=True) + EPS)
        gate = og_ref[:, span].astype(F32)
        gate = gate * jax.nn.sigmoid(gate)
        rec.append((out * scale * hgain_ref[...].astype(F32) * gate).astype(BF16))
    rec = jnp.concatenate(rec, axis=1)
    mixed = mixed_ref[...]
    behind = jnp.maximum(at - 1, 0)
    lines = jnp.concatenate(
        [enter_ref[behind, n].astype(F32) for n in range(heads, enter_ref.shape[1])], axis=0
    )
    taken = CK - 1
    rim = jnp.concatenate(
        [
            lines[2 * taken * h : 2 * taken * h + taken] + lines[2 * taken * h + taken : 2 * taken * (h + 1)]
            for h in range(heads)
        ],
        axis=1,
    )
    rim = jnp.concatenate([jnp.zeros((8 - taken, width), F32), rim], axis=0)
    rim = jnp.where(at == 0, 0.0, rim)
    edge = jnp.where(b == 0, rim, edge_ref[...])
    padded = jnp.concatenate([edge, mixed], axis=0)
    taps = taps_ref[...].astype(F32)
    base = edge.shape[0] - (CK - 1)
    conv = padded[base : base + block] * taps[0:1]
    for j in range(1, CK):
        conv = conv + padded[base + j : base + j + block] * taps[j : j + 1]
    conv = (post_ref[...].astype(F32) * conv).astype(BF16)

    @pl.when(i == 0)
    def _():
        for copy in copies:
            copy.wait()

    result = (
        jnp.dot(rec, wr_ref[...], preferred_element_type=F32)
        + jnp.dot(conv, wc_ref[...], preferred_element_type=F32)
    ).astype(BF16)
    for n in range(outputs):

        @pl.when(i == n)
        def _():
            outs[n][...] = result


def shards(
    layer_input,
    input_norm_gain,
    query_weight,
    forget_weight,
    value_matrix,
    output_gate_weight,
    after_gate_weight,
    before_gate_weight,
    convolution_input_weight,
    forget_minimum,
    surge_log_decay,
    convolution_kernel,
    head_norm_gain,
    starting_state,
    recurrence_output_weight,
    convolution_output_weight,
    output_norm_gain,
):
    tokens, piece = layer_input.shape
    features, width = query_weight.shape
    heads = width // DK
    tp = lax.axis_size("tp")
    sp = lax.axis_size("sp")
    me = lax.axis_index("tp")
    at = lax.axis_index("sp")
    block = tokens // tp
    blocks = tp

    chunks = 2
    span = tokens // chunks
    chunk_blocks = span // block
    sds = jax.ShapeDtypeStruct

    parts = [layer_input[n * span : (n + 1) * span] for n in range(chunks)]
    held = [[part] for part in parts]
    order = [0]
    bit = tp // 2
    while bit:
        held = [row + [xor_permute(x, "tp", bit) for x in row] for row in held]
        order = order + [m | bit for m in order]
        bit //= 2
    ids = jnp.stack([me ^ m for m in order]).astype(jnp.int32)

    rows_each = DV // sp
    full_start = lax.all_gather(starting_state, "sp", axis=1, tiled=True)
    start_rows = lax.dynamic_slice_in_dim(full_start, at * rows_each, rows_each, axis=2)
    start_rows = start_rows.transpose(0, 2, 1)

    weights = {
        "forget": forget_weight,
        "value": value_matrix,
        "before": before_gate_weight,
        "convin": convolution_input_weight,
        "query": query_weight,
        "outgate": output_gate_weight,
        "after": after_gate_weight,
    }
    whole = lambda shape: pl.BlockSpec(shape, lambda i: (0,) * len(shape))
    part_of = lambda n, rest: pl.BlockSpec((span, rest), lambda i, n=n: (n, 0))

    def hbm(names):
        return {"hbm_" + w: (weights[w], ANY) for w in names}

    def bufs(names):
        spaces = {"buf_" + w: pltpu.VMEM((features, width), BF16) for w in names}
        spaces["sems"] = pltpu.SemaphoreType.DMA((len(names),))
        return spaces

    def norm_inputs(n):
        taken = {"ids": (ids, SMEM)}
        for j, x in enumerate(held[n]):
            taken["x%d" % j] = (x, whole((span, piece)))
        taken["gain"] = (input_norm_gain.reshape(tp, 1, piece), whole((tp, 1, piece)))
        taken["minimum"] = (forget_minimum.reshape(1, width), whole((1, width)))
        taken["surge"] = (surge_log_decay, part_of(n, width))
        return taken

    def outputs_of(n, names):
        return {
            w: (sds((tokens, width), F32 if w in ("keys", "decay", "mixed") else BF16), part_of(n, width))
            for w in names
        }

    def state_outputs(n):
        taken = outputs_of(n, ("value", "keys", "decay"))
        taken["pre"] = (
            sds((blocks, heads, DV, DK), F32),
            pl.BlockSpec((chunk_blocks, heads, DV, DK), lambda i: (n, 0, 0, 0)),
        )
        taken["predecay"] = (
            sds((blocks, 1, width), F32),
            pl.BlockSpec((chunk_blocks, 1, width), lambda i: (n, 0, 0)),
        )
        return taken

    def before_and_convin(r, copies):
        r.mixed[...] = project(r, copies, "before").astype(F32)
        r.mixed[...] = r.mixed[...] * project(r, copies, "convin").astype(F32)

    def first_body(r):
        copies = weight_copies(r, weights)
        norm_piece(r, tp)
        forget_value_state(r, copies, block, True, False)
        before_and_convin(r, copies)
        for w in ("query", "outgate", "after"):
            r.get(w)[...] = project(r, copies, w)

    full = named_call(
        first_body,
        "first",
        {**norm_inputs(0), **hbm(weights)},
        {
            **state_outputs(0),
            **outputs_of(0, ("mixed", "query", "outgate", "after")),
            "carry_out": (sds((heads, DV, DK), F32), whole((heads, DV, DK))),
            "carry_decay_out": (sds((1, width), F32), whole((1, width))),
        },
        {
            **bufs(weights),
            "normed": pltpu.VMEM((span, features), BF16),
            "forget": pltpu.VMEM((span, width), BF16),
        },
    )

    def second_body(r):
        copies = weight_copies(r, ("forget", "value"))
        norm_piece(r, tp)
        forget_value_state(r, copies, block, False, True)

    slabs = heads + -(-2 * heads // rows_each)
    kept = ("value", "keys", "decay", "pre", "predecay")
    second = named_call(
        second_body,
        "second",
        {
            **norm_inputs(1),
            **hbm(("forget", "value")),
            "carry": (full["carry_out"], whole((heads, DV, DK))),
            "carry_decay": (full["carry_decay_out"], whole((1, width))),
            **{"old_" + w: (full[w], ANY) for w in kept},
        },
        {
            **state_outputs(1),
            "pack": (sds((sp, slabs, rows_each, DK), BF16), whole((sp, slabs, rows_each, DK))),
            "normed": (sds((span, features), BF16), whole((span, features))),
        },
        {**bufs(("forget", "value")), "forget": pltpu.VMEM((span, width), BF16)},
        {"old_" + w: w for w in kept},
    )
    full.update({w: second[w] for w in kept})
    normed = second["normed"]
    moved = lax.all_to_all(second["pack"], "sp", split_axis=0, concat_axis=0, tiled=True)

    def mixed_body(r):
        before_and_convin(r, weight_copies(r, ("before", "convin")))

    full["mixed"] = named_call(
        mixed_body,
        "convin",
        {
            "normed": (normed, whole((span, features))),
            **hbm(("before", "convin")),
            "old_mixed": (full["mixed"], ANY),
        },
        outputs_of(1, ("mixed",)),
        bufs(("before", "convin")),
        {"old_mixed": "mixed"},
    )["mixed"]

    extra = -(-2 * (CK - 1) * heads // rows_each)
    enter = named_call(
        functools.partial(advance_kernel, heads=heads),
        "advance",
        {
            "moved": (moved, whole((sp, slabs, rows_each, DK))),
            "start": (start_rows, whole((heads, rows_each, DK))),
            "mixed": (full["mixed"], pl.BlockSpec((8, width), lambda i: (tokens // 8 - 1, 0))),
        },
        {
            "enter": (
                sds((sp, heads + extra, rows_each, DK), BF16),
                whole((sp, heads + extra, rows_each, DK)),
            )
        },
        {},
    )["enter"]
    normed, enter = lax.optimization_barrier((normed, enter))
    enter = lax.all_to_all(enter, "sp", split_axis=0, concat_axis=0, tiled=True)

    def rest_body(r):
        copies = weight_copies(r, ("query", "outgate", "after"))
        for w in ("query", "outgate", "after"):
            r.get(w)[...] = project(r, copies, w)

    rest = ("query", "outgate", "after")
    full.update(
        named_call(
            rest_body,
            "rest",
            {
                "normed": (normed, whole((span, features))),
                **hbm(rest),
                **{"old_" + w: (full[w], ANY) for w in rest},
            },
            outputs_of(1, rest),
            bufs(rest),
            {"old_" + w: w for w in rest},
        )
    )

    half = tp // 2
    rows8 = block // 8

    def mix(block_ids):
        count = len(block_ids)
        at_block = lambda i, ids: (ids[i], 0)
        whole = lambda *shape: pl.BlockSpec(shape, lambda i, ids: (0,) * len(shape))
        tile = pl.BlockSpec((block, width), at_block)
        return pl.pallas_call(
            functools.partial(mix_kernel, count),
            grid_spec=pltpu.PrefetchScalarGridSpec(
                num_scalar_prefetch=1,
                grid=(count,),
                in_specs=[
                    tile, tile, tile, tile, tile, tile, tile,
                    pl.BlockSpec((8, width), lambda i, ids: (jnp.maximum(ids[i] * rows8 - 1, 0), 0)),
                    whole(CK, width),
                    whole(1, DV),
                    whole(sp, heads + extra, rows_each, DK),
                    pl.BlockSpec((1, heads, DV, DK), lambda i, ids: (ids[i], 0, 0, 0)),
                    pl.BlockSpec((1, 1, width), lambda i, ids: (ids[i], 0, 0)),
                    ANY,
                    ANY,
                ],
                scratch_shapes=[
                    pltpu.VMEM((width, features), BF16),
                    pltpu.VMEM((width, features), BF16),
                    pltpu.SemaphoreType.DMA((2,)),
                ],
                out_specs=[whole(block, features)] * count,
            ),
            out_shape=[sds((block, features), BF16)] * count,
            compiler_params=pltpu.CompilerParams(vmem_limit_bytes=56 * 1024 * 1024),
            name="mix",
        )(
            jnp.stack(list(block_ids) + [at]).astype(jnp.int32),
            full["query"], full["keys"], full["decay"], full["value"], full["outgate"],
            full["after"], full["mixed"], full["mixed"],
            convolution_kernel, head_norm_gain.reshape(1, DV), enter, full["pre"], full["predecay"],
            recurrence_output_weight, convolution_output_weight,
        )

    def fold(parts):
        parts = list(parts)
        step = len(parts) // 2
        bit = 1
        while step:
            moved = [xor_permute(parts[m], "tp", bit) for m in range(1, len(parts), 2)]
            parts = [
                (parts[2 * n].astype(F32) + moved[n].astype(F32)).astype(BF16)
                for n in range(step)
            ]
            step //= 2
            bit *= 2
        return parts[0]

    away = fold(mix([me ^ (half + m) for m in range(half)]))
    away, later = lax.optimization_barrier((away, me))
    arrived = xor_permute(away, "tp", half)
    home = fold(mix([later ^ m for m in range(half)]))
    mixed = home.astype(F32) + arrived.astype(F32)
    scale = lax.rsqrt(jnp.mean(mixed * mixed, axis=-1, keepdims=True) + EPS)
    return (mixed * scale * output_norm_gain.astype(F32)).astype(BF16)


def solution(mesh):
    return jax.shard_map(
        shards,
        mesh=mesh,
        in_specs=(
            P("sp", "tp"),
            P(),
            P(None, "tp"),
            P(None, "tp"),
            P(None, "tp"),
            P(None, "tp"),
            P(None, "tp"),
            P(None, "tp"),
            P(None, "tp"),
            P("tp"),
            P("sp", "tp"),
            P(None, "tp"),
            P(),
            P("tp", "sp", None),
            P("tp", None),
            P("tp", None),
            P(),
        ),
        out_specs=P(("sp", "tp"), None),
        check_vma=False,
    )
```

time: 142 us -> 146 us (1.028)
  blocking collectives: 0 us -> 32.3 us
  waiting for transfers between devices: 54.7 us -> 25.7 us
  between operations: 13.5 us -> 0.24 us
  starting transfers between devices: 8.79 us -> 16.1 us
  Pallas kernels: 52.3 us -> 58.8 us
  local copies, waits for them, and re-layouts: 3.71 us -> 5.92 us
  other arithmetic: 8.13 us -> 6.3 us
    all_gather x0 -> x1, blocking collectives: none -> 32.3 us  [shards(): full_start = lax.all_gather(starting_state, 'sp', axis=1, tiled=True)]
    all_gather x1 -> x0, waiting for transfers between devices: 18.6 us -> none  [shards(): every = lax.all_gather(pack, 'sp', axis=0, tiled=False)]
    ppermute x6 -> x9, waiting for transfers between devices: 36.1 us -> 25.5 us  [xor_permute(): return lax.ppermute(value, axis, [(i, i ^ bit) for i in range(peers)])]
    all_to_all x0 -> x2, starting transfers between devices: none -> 10.6 us  [the longest x1 6.09 us: shards(): lax.all_to_all(second['pack'], 'sp', split_axis=0, concat_axis=0, tiled=T...]
    ppermute x1 -> x0, starting transfers between devices: 3.66 us -> none  [from_behind(): lax.ppermute(value, axis, [(i, i + by) for i in range(peers) if 0 <= i +...]
    pallas_call x3 -> x5, Pallas kernels: 33.4 us -> 36.9 us  [named_call(): pl.pallas_call(kernel, grid=(1,), out_shape=[shape for shape, _ in outs.v...]
    pallas_call x2, Pallas kernels: 18.9 us -> 21.9 us  [mix(): pl.pallas_call(functools.partial(mix_kernel, count), grid_spec=pltpu.Pref...]
    unnamed x14 -> x30, local copies, waits for them, and re-layouts: 1.52 us -> 3.88 us
  transfers between devices with their start and end apart: 8 -> 11, of which waited for: 5 -> 5; matrix products, arithmetic and copies ran while one was open for 6% -> 2% of each run, Pallas kernels for 21% -> 26%
where the time goes in v2:
time: 146 us; the launch traced here: 145 us
  Pallas kernels  58.8 us (40%)
  blocking collectives  32.3 us (22%)
  waiting for transfers between devices  25.7 us (18%)
  starting transfers between devices  16.1 us (11%)
  other arithmetic  6.3 us (4%)
  local copies, waits for them, and re-layouts  5.92 us (4%)
    pallas_call x5, Pallas kernels, named_call(): pl.pallas_call(kernel, grid=(1,), out_shape=[shape for shape, _ in outs.v...  36.9 us
    all_gather x1, blocking collectives, shards(): full_start = lax.all_gather(starting_state, 'sp', axis=1, tiled=True)  32.3 us
    ppermute x9, waiting for transfers between devices, xor_permute(): return lax.ppermute(value, axis, [(i, i ^ bit) for i in range(peers)])  25.5 us
    pallas_call x2, Pallas kernels, mix(): pl.pallas_call(functools.partial(mix_kernel, count), grid_spec=pltpu.Pref...  21.9 us
    all_to_all x1, starting transfers between devices, shards(): lax.all_to_all(second['pack'], 'sp', split_axis=0, concat_axis=0, tiled=T...  6.09 us
    ppermute x9, starting transfers between devices, xor_permute(): return lax.ppermute(value, axis, [(i, i ^ bit) for i in range(peers)])  5.47 us
    all_to_all x1, starting transfers between devices, shards(): enter = lax.all_to_all(enter, 'sp', split_axis=0, concat_axis=0, tiled=True)  4.53 us
    unnamed x30, local copies, waits for them, and re-layouts  3.88 us
  transfers between devices with their start and end apart: 11, of which 5 were waited for; matrix products, arithmetic and copies ran while one was open for 2% of the time, Pallas kernels for 26%

profile of v2, /device:TPU:0, one launch (start us, length us, event | category | flops | bytes accessed | tf_op | source)
XLA Modules:
  0.0 145.3 jit_solution(11414258283354765707)
XLA Ops:
  0.0 1.2 fusion
  1.2 0.0 copy-start.2
  1.2 0.0 copy-start.1
  1.2 3.0 %collective-permute-start.3 = (bf16[384,512]{1,0:T(8,128)(2,1)S(1)}, bf16[384,512]{1,0:T(8,128)(2,1)S(1)}, u32[]{:S(2)}, u32[]{:S(2)}) collective-permute-start(bf16[384,512]{1,0:T(8,128)(2,1)S(1)} %get-tuple-element.63.refs_1_), channel_id=1, source_target_pairs={{0,2},{1,3},{2,0},{3,1},{4,6},{5,7},{6,4},{7,5},{8,10},{9,11},{10,... | collective-permute-start | bytes 1179656 | tf_op jit(solution)/shard_map/ppermute | solution.py:22
  4.2 0.1 collective-permute-start
  4.3 0.0 collective-permute-start.4
  4.3 9.9 %collective-permute-done.3.refs_2_ = bf16[384,512]{1,0:T(8,128)(2,1)S(1)} collective-permute-done((bf16[384,512]{1,0:T(8,128)(2,1)S(1)}, bf16[384,512]{1,0:T(8,128)(2,1)S(1)}, u32[]{:S(2)}, u32[]{:S(2)}) %collective-permute-start.3) | collective-permute-done | bytes 393248 | tf_op jit(solution)/shard_map/ppermute | solution.py:22
  14.2 0.0 collective-permute-start.5
  14.2 0.5 collective-permute-start.1
  14.7 7.1 %collective-permute-done.refs_2_ = bf16[384,512]{1,0:T(8,128)(2,1)S(1)} collective-permute-done((bf16[384,512]{1,0:T(8,128)(2,1)S(1)}, bf16[384,512]{1,0:T(8,128)(2,1)S(1)}, u32[]{:S(2)}, u32[]{:S(2)}) %collective-permute-start) | collective-permute-done | bytes 393248 | tf_op jit(solution)/shard_map/ppermute | solution.py:22
  21.8 0.0 collective-permute-start.2
  21.8 0.7 reshape.24.refs_5_
  22.4 0.6 pad_add_fusion.refs_0_
  23.1 0.0 collective-permute-done.4.refs_3_
  23.1 0.0 collective-permute-done.5.refs_4_
  23.1 0.7 copy-done.9
  23.8 0.2 copy-done.10
  24.0 13.7 %first.1 = (bf16[768,512]{1,0:T(8,128)(2,1)}, f32[768,512]{1,0:T(8,128)}, f32[768,512]{1,0:T(8,128)}, f32[4,4,128,128]{3,2,1,0:T(8,128)}, f32[4,1,512]{2,1,0:T(1...) custom-call(s32[4]{0:T(128)} %pad_add_fusion.refs_0_, ...), custom_call_target="tpu_custom_call" | custom-call | tf_op jit(solution)/shard_map/first/pallas_call | solution.py:49
  37.7 0.0 collective-permute-done.1.refs_3_
  37.8 0.0 collective-permute-done.2.refs_4_
  37.8 0.7 copy-done.6
  38.5 0.1 copy-done.7
  38.7 9.0 %second.1 = (bf16[768,512]{1,0:T(8,128)(2,1)}, f32[768,512]{1,0:T(8,128)}, f32[768,512]{1,0:T(8,128)}, f32[4,4,128,128]{3,2,1,0:T(8,128)}, f32[4,1,512]{2,1,0:T(...) custom-call(s32[4]{0:T(128)} %pad_add_fusion.refs_0_, ...), custom_call_target="tpu_custom_call", output_to_operand_aliasing={{0}: (12, {}), {1}: (13, {}), {2}: (14, {}), {3}: (15, {}),... | custom-call | tf_op jit(solution)/shard_map/second/pallas_call | solution.py:49
  47.6 6.1 %all-to-all-start = ((bf16[8,5,16,128]{3,2,1,0:T(8,128)(2,1)}), bf16[8,5,16,128]{3,2,1,0:T(8,128)(2,1)S(1)}, u32[]{:S(2)}, u32[]{:S(2)}) async-start(bf16[8,5,16,128]{3,2,1,0:T(8,128)(2,1)} %get-tuple-element.42), calls=%async_computation | async-start | bytes 327680 | tf_op jit(solution)/shard_map/all_to_all | solution.py:426
  53.8 32.3 %all_gather.3 = f32[4,128,128]{2,0,1:T(4,128)S(1)} all-gather(f32[4,16,128]{2,0,1:T(4,128)S(1)} %copy.33), channel_id=1, replica_groups=mesh['sp'=8,'tp'=4] {'sp'}, dimensions={1}, use_global_device_ids=true | all-gather | bytes 294912 | tf_op jit(solution)/shard_map/all_gather | solution.py:319
  86.1 0.2 constant_dynamic-slice_fusion
  86.3 0.7 copy.35
  87.0 5.9 %convin.1.refs_2_.refs_6_.refs_7_ = f32[768,512]{1,0:T(8,128)} custom-call(bf16[384,2048]{1,0:T(8,128)(2,1)} %get-tuple-element.44.refs_0_, bf16[2048,512]{1,0:T(8,128)(2,1)} %refs_1_.2, bf16[2048,512]{1,0:T(8,128)(2,1)} %refs_2_.2, f32[768,512]{1,0:T(8,128)} %get-tuple-element.43.refs_3_), custom_call_target="tpu_custom_call", output_to_operand_aliasing={{}: (3, {})} | custom-call | tf_op jit(solution)/shard_map/convin/pallas_call | solution.py:49
  92.9 0.0 all-to-all-done.refs_0_
  92.9 0.6 copy-done.4
  93.5 1.7 %advance.1 = bf16[8,5,16,128]{3,2,1,0:T(8,128)(2,1)} custom-call(bf16[8,5,16,128]{3,2,1,0:T(8,128)(2,1)} %copy-done.4, f32[4,16,128]{2,1,0:T(8,128)} %bitcast.10, f32[768,512]{1,0:T(8,128)} %convin.1.refs_2_.refs_6_.refs_7_), custom_call_target="tpu_custom_call" | custom-call | tf_op jit(solution)/shard_map/advance/pallas_call | solution.py:49
  95.2 4.5 %all-to-all-start.1 = ((bf16[8,5,16,128]{3,2,1,0:T(8,128)(2,1)}), bf16[8,5,16,128]{3,2,1,0:T(8,128)(2,1)S(1)}, u32[]{:S(2)}, u32[]{:S(2)}) async-start(bf16[8,5,16,128]{3,2,1,0:T(8,128)(2,1)} %advance.1), calls=%async_computation.1 | async-start | bytes 327680 | tf_op jit(solution)/shard_map/all_to_all | solution.py:462
  99.7 0.7 add_add_fusion.ids_ref
  100.4 6.7 %rest.1 = (bf16[768,512]{1,0:T(8,128)(2,1)}, bf16[768,512]{1,0:T(8,128)(2,1)}, bf16[768,512]{1,0:T(8,128)(2,1)}) custom-call(bf16[384,2048]{1,0:T(8,128)(2,1)} %get-tuple-element.44.refs_0_, bf16[2048,512]{1,0:T(8,128)(2,1)} %refs_1_.3, bf16[2048,512]{1,0:T(8,128)(2,1)} %refs_2_.3, ...), custom_call_target="tpu_custom_call", output_to_operand_aliasing={{0}: (4, {}), {1}: (5, {}), {2}: (6, {})} | custom-call | tf_op jit(solution)/shard_map/rest/pallas_call | solution.py:49
  107.1 0.2 all-to-all-done.1.refs_10_
  107.3 0.7 copy-done.3
  108.0 10.8 %mix.2 = (bf16[192,2048]{1,0:T(8,128)(2,1)}, bf16[192,2048]{1,0:T(8,128)(2,1)}) custom-call(s32[3]{0:T(128)} %add_add_fusion.ids_ref, bf16[768,512]{1,0:T(8,128)(2,1)} %get-tuple-element.48.refs_0_, f32[768,512]{1,0:T(8,128)} %get-tuple-element.49.refs_1_, f32[768,512]{1,0:T(8,128)} %get-tuple-element.50.refs_2_, ...), custom_call_target="tpu_custom_call" | custom-call | tf_op jit(solution)/shard_map/mix/pallas_call | solution.py:493
  118.8 0.1 collective-permute-start.6
  118.9 2.5 %collective-permute-done.6 = bf16[192,2048]{1,0:T(8,128)(2,1)S(1)} collective-permute-done((bf16[192,2048]{1,0:T(8,128)(2,1)}, bf16[192,2048]{1,0:T(8,128)(2,1)S(1)}, u32[]{:S(2)}, u32[]{:S(2)}) %collective-permute-start.6) | collective-permute-done | bytes 786464 | tf_op jit(solution)/shard_map/ppermute | solution.py:22
  121.3 1.4 add_convert_fusion.1
  122.7 1.7 %collective-permute-start.8 = (bf16[192,2048]{1,0:T(8,128)(2,1)S(1)}, bf16[192,2048]{1,0:T(8,128)(2,1)S(1)}, u32[]{:S(2)}, u32[]{:S(2)}) collective-permute-start(bf16[192,2048]{1,0:T(8,128)(2,1)S(1)} %add_convert_fusion.1), channel_id=1, source_target_pairs={{0,2},{1,3},{2,0},{3,1},{4,6},{5,7},{6,4},{7,5},{8,10},{9,11},{10,... | collective-permute-start | bytes 2359304 | tf_op jit(solution)/shard_map/ppermute | solution.py:22
  124.5 0.7 add_add_fusion.1.ids_ref
  125.1 11.1 %mix.3 = (bf16[192,2048]{1,0:T(8,128)(2,1)}, bf16[192,2048]{1,0:T(8,128)(2,1)}) custom-call(s32[3]{0:T(128)} %add_add_fusion.1.ids_ref, bf16[768,512]{1,0:T(8,128)(2,1)} %get-tuple-element.48.refs_0_, f32[768,512]{1,0:T(8,128)} %get-tuple-element.49.refs_1_, f32[768,512]{1,0:T(8,128)} %get-tuple-element.50.refs_2_, ...), custom_call_target="tpu_custom_call" | custom-call | tf_op jit(solution)/shard_map/mix/pallas_call | solution.py:493
  136.2 0.1 collective-permute-start.7
  136.3 6.1 %collective-permute-done.8 = bf16[192,2048]{1,0:T(8,128)(2,1)S(1)} collective-permute-done((bf16[192,2048]{1,0:T(8,128)(2,1)S(1)}, bf16[192,2048]{1,0:T(8,128)(2,1)S(1)}, u32[]{:S(2)}, u32[]{:S(2)}) %collective-permute-start.8) | collective-permute-done | bytes 786464 | tf_op jit(solution)/shard_map/ppermute | solution.py:22
  142.4 0.0 collective-permute-done.7
  142.4 1.6 %multiply_reduce_fusion = f32[192]{0:T(256)S(1)} fusion(bf16[192,2048]{1,0:T(8,128)(2,1)S(1)} %collective-permute-done.8, bf16[192,2048]{1,0:T(8,128)(2,1)S(1)} %collective-permute-done.7, bf16[192,2048]{1,0:T(8,128)(2,1)} %get-tuple-element.60), kind=kLoop, calls=%fused_computation.1 | loop fusion | flops 3538752 | bytes 2360064 | tf_op jit(solution)/shard_map/reduce_sum | solution.py:546
  144.0 1.4 multiply_convert_fusion
  (23 shorter events, 0.1 us)
Async XLA Ops:
  0.0 21.8 %copy-start.12 = (bf16[2048]{0:T(1024)(128)(2,1)S(1)}, bf16[2048]{0:T(1024)(128)(2,1)}, u32[]{:S(2)}) copy-start(bf16[2048]{0:T(1024)(128)(2,1)} %param.18) | copy-start | bytes 12292
  1.2 21.9 %copy-start.2 = (bf16[384,512]{1,0:T(8,128)(2,1)}, bf16[384,512]{1,0:T(8,128)(2,1)S(1)}, u32[]{:S(2)}) copy-start(bf16[384,512]{1,0:T(8,128)(2,1)S(1)} %get-tuple-element.63.refs_1_) | copy-start | bytes 1179652
  1.2 36.5 %copy-start.1 = (bf16[384,512]{1,0:T(8,128)(2,1)}, bf16[384,512]{1,0:T(8,128)(2,1)S(1)}, u32[]{:S(2)}) copy-start(bf16[384,512]{1,0:T(8,128)(2,1)S(1)} %get-tuple-element.64.refs_1_) | copy-start | bytes 1179652
  1.2 13.0 %collective-permute-start.3 = (bf16[384,512]{1,0:T(8,128)(2,1)S(1)}, bf16[384,512]{1,0:T(8,128)(2,1)S(1)}, u32[]{:S(2)}, u32[]{:S(2)}) collective-permute-start(bf16[384,512]{1,0:T(8,128)(2,1)S(1)} %get-tuple-element.63.refs_1_), channel_id=1, source_target_pairs={{0,2},{1,3},{2,0},{3,1},{4,6},{5,7},{6,4},{7,5},{8,10},{9,11},{10,... | collective-permute-start | bytes 1179656 | tf_op jit(solution)/shard_map/ppermute | solution.py:22
  4.2 17.5 %collective-permute-start = (bf16[384,512]{1,0:T(8,128)(2,1)S(1)}, bf16[384,512]{1,0:T(8,128)(2,1)S(1)}, u32[]{:S(2)}, u32[]{:S(2)}) collective-permute-start(bf16[384,512]{1,0:T(8,128)(2,1)S(1)} %get-tuple-element.64.refs_1_), channel_id=1, source_target_pairs={{0,2},{1,3},{2,0},{3,1},{4,6},{5,7},{6,4},{7,5},{8,10},{9,11},{10,... | collective-permute-start | bytes 1179656 | tf_op jit(solution)/shard_map/ppermute | solution.py:22
  4.3 18.8 %collective-permute-start.4 = (bf16[384,512]{1,0:T(8,128)(2,1)S(1)}, bf16[384,512]{1,0:T(8,128)(2,1)S(1)}, u32[]{:S(2)}, u32[]{:S(2)}) collective-permute-start(bf16[384,512]{1,0:T(8,128)(2,1)S(1)} %get-tuple-element.63.refs_1_), channel_id=1, source_target_pairs={{0,1},{1,0},{2,3},{3,2},{4,5},{5,4},{6,7},{7,6},{8,9},{9,8},{10,11... | collective-permute-start | bytes 1179656 | tf_op jit(solution)/shard_map/ppermute | solution.py:22
  14.2 8.9 %copy-start.8 = (bf16[384,512]{1,0:T(8,128)(2,1)}, bf16[384,512]{1,0:T(8,128)(2,1)S(1)}, u32[]{:S(2)}) copy-start(bf16[384,512]{1,0:T(8,128)(2,1)S(1)} %collective-permute-done.3.refs_2_) | copy-start | bytes 1179652
  14.2 8.9 %collective-permute-start.5 = (bf16[384,512]{1,0:T(8,128)(2,1)S(1)}, bf16[384,512]{1,0:T(8,128)(2,1)S(1)}, u32[]{:S(2)}, u32[]{:S(2)}) collective-permute-start(bf16[384,512]{1,0:T(8,128)(2,1)S(1)} %collective-permute-done.3.refs_2_), channel_id=1, source_target_pairs={{0,1},{1,0},{2,3},{3,2},{4,5},{5,4},{6,7},{7,6},{8,9},{9,8},{10,11... | collective-permute-start | bytes 1179656 | tf_op jit(solution)/shard_map/ppermute | solution.py:22
  14.2 23.5 %collective-permute-start.1 = (bf16[384,512]{1,0:T(8,128)(2,1)S(1)}, bf16[384,512]{1,0:T(8,128)(2,1)S(1)}, u32[]{:S(2)}, u32[]{:S(2)}) collective-permute-start(bf16[384,512]{1,0:T(8,128)(2,1)S(1)} %get-tuple-element.64.refs_1_), channel_id=1, source_target_pairs={{0,1},{1,0},{2,3},{3,2},{4,5},{5,4},{6,7},{7,6},{8,9},{9,8},{10,11... | collective-permute-start | bytes 1179656 | tf_op jit(solution)/shard_map/ppermute | solution.py:22
  21.8 16.0 %copy-start.5 = (bf16[384,512]{1,0:T(8,128)(2,1)}, bf16[384,512]{1,0:T(8,128)(2,1)S(1)}, u32[]{:S(2)}) copy-start(bf16[384,512]{1,0:T(8,128)(2,1)S(1)} %collective-permute-done.refs_2_) | copy-start | bytes 1179652
  21.8 16.0 %collective-permute-start.2 = (bf16[384,512]{1,0:T(8,128)(2,1)S(1)}, bf16[384,512]{1,0:T(8,128)(2,1)S(1)}, u32[]{:S(2)}, u32[]{:S(2)}) collective-permute-start(bf16[384,512]{1,0:T(8,128)(2,1)S(1)} %collective-permute-done.refs_2_), channel_id=1, source_target_pairs={{0,1},{1,0},{2,3},{3,2},{4,5},{5,4},{6,7},{7,6},{8,9},{9,8},{10,11... | collective-permute-start | bytes 1179656 | tf_op jit(solution)/shard_map/ppermute | solution.py:22
  23.1 0.8 copy-start.9
  23.1 0.9 copy-start.10
  37.7 0.8 copy-start.6
  37.8 0.9 copy-start.7
  38.7 15.1 %copy-start.11 = (f32[4,16,128]{2,1,0:T(8,128)S(1)}, f32[4,16,128]{2,1,0:T(8,128)}, u32[]{:S(2)}) copy-start(f32[4,16,128]{2,1,0:T(8,128)} %param.30) | copy-start | bytes 98308
  47.6 45.2 %all-to-all-start = ((bf16[8,5,16,128]{3,2,1,0:T(8,128)(2,1)}), bf16[8,5,16,128]{3,2,1,0:T(8,128)(2,1)S(1)}, u32[]{:S(2)}, u32[]{:S(2)}) async-start(bf16[8,5,16,128]{3,2,1,0:T(8,128)(2,1)} %get-tuple-element.42), calls=%async_computation | async-start | bytes 327680 | tf_op jit(solution)/shard_map/all_to_all | solution.py:426
  92.9 0.7 copy-start.4
  95.2 12.1 %all-to-all-start.1 = ((bf16[8,5,16,128]{3,2,1,0:T(8,128)(2,1)}), bf16[8,5,16,128]{3,2,1,0:T(8,128)(2,1)S(1)}, u32[]{:S(2)}, u32[]{:S(2)}) async-start(bf16[8,5,16,128]{3,2,1,0:T(8,128)(2,1)} %advance.1), calls=%async_computation.1 | async-start | bytes 327680 | tf_op jit(solution)/shard_map/all_to_all | solution.py:462
  107.3 0.7 copy-start.3
  118.8 2.6 %collective-permute-start.6 = (bf16[192,2048]{1,0:T(8,128)(2,1)}, bf16[192,2048]{1,0:T(8,128)(2,1)S(1)}, u32[]{:S(2)}, u32[]{:S(2)}) collective-permute-start(bf16[192,2048]{1,0:T(8,128)(2,1)} %get-tuple-element.58), channel_id=1, source_target_pairs={{0,1},{1,0},{2,3},{3,2},{4,5},{5,4},{6,7},{7,6},{8,9},{9,8},{10,11... | collective-permute-start | bytes 2359304 | tf_op jit(solution)/shard_map/ppermute | solution.py:22
  122.7 19.6 %collective-permute-start.8 = (bf16[192,2048]{1,0:T(8,128)(2,1)S(1)}, bf16[192,2048]{1,0:T(8,128)(2,1)S(1)}, u32[]{:S(2)}, u32[]{:S(2)}) collective-permute-start(bf16[192,2048]{1,0:T(8,128)(2,1)S(1)} %add_convert_fusion.1), channel_id=1, source_target_pairs={{0,2},{1,3},{2,0},{3,1},{4,6},{5,7},{6,4},{7,5},{8,10},{9,11},{10,... | collective-permute-start | bytes 2359304 | tf_op jit(solution)/shard_map/ppermute | solution.py:22
  125.1 11.2 %copy-start.13 = (bf16[2048]{0:T(1024)(128)(2,1)S(1)}, bf16[2048]{0:T(1024)(128)(2,1)}, u32[]{:S(2)}) copy-start(bf16[2048]{0:T(1024)(128)(2,1)} %param.33) | copy-start | bytes 12292
  136.2 7.8 %copy-start = (bf16[192,2048]{1,0:T(8,128)(2,1)S(1)}, bf16[192,2048]{1,0:T(8,128)(2,1)}, u32[]{:S(2)}) copy-start(bf16[192,2048]{1,0:T(8,128)(2,1)} %get-tuple-element.60) | copy-start | bytes 2359300
  136.2 6.2 %collective-permute-start.7 = (bf16[192,2048]{1,0:T(8,128)(2,1)}, bf16[192,2048]{1,0:T(8,128)(2,1)S(1)}, u32[]{:S(2)}, u32[]{:S(2)}) collective-permute-start(bf16[192,2048]{1,0:T(8,128)(2,1)} %get-tuple-element.61), channel_id=1, source_target_pairs={{0,1},{1,0},{2,3},{3,2},{4,5},{5,4},{6,7},{7,6},{8,9},{9,8},{10,11... | collective-permute-start | bytes 2359304 | tf_op jit(solution)/shard_map/ppermute | solution.py:22
